TPU v7x, 32 devices: a whole 2x2x4 slice. The times are simulated.
32 devices in a mesh: fs: 4 (over y, x), tp: 8 (over z, core).
Axes of the slice: x: 2, y: 2, z: 4, core: 2. Of those that a mesh axis runs over, the one named last changes fastest.
Arguments:
- value_input: bfloat16 [8192, 2048], P('fs', 'tp'), may hold values from -50 to 50
- value_cotangent: bfloat16 [8192, 512], P('fs'), may hold values from -6 to 6
- value_factor: bfloat16 [512, 128], replicated, may hold values from -10 to 10
- value_master: float32 [512, 2048], P('fs', 'tp'), may hold values from -0.125 to 0.125
- value_first: float32 [128, 2048], P('fs', 'tp'), may hold values from -4 to 4
- value_second: float32 [128, 2048], P('fs', 'tp'), may hold values from 0.01 to 0.2
- mixed_heads: bfloat16 [8192, 1024], P('fs', 'tp'), may hold values from -6 to 6
- output_cotangent: bfloat16 [8192, 2048], P('fs', 'tp'), may hold values from -50 to 50
- output_factor: bfloat16 [1024, 128], replicated, may hold values from -10 to 10
- output_master: float32 [1024, 2048], P('fs', 'tp'), may hold values from -0.1875 to 0.1875
- output_first: float32 [128, 2048], P('fs', 'tp'), may hold values from -4 to 4
- output_second: float32 [128, 2048], P('fs', 'tp'), may hold values from 0.01 to 0.2
Outputs:
- value_step: float32 [512, 2048], P('fs', 'tp')
- value_new_master: float32 [512, 2048], P('fs', 'tp')
- value_copy: bfloat16 [512, 2048], P(None, 'tp')
- value_first_new: float32 [128, 2048], P('fs', 'tp')
- value_second_new: float32 [128, 2048], P('fs', 'tp')
- output_step: float32 [1024, 2048], P('fs', 'tp')
- output_new_master: float32 [1024, 2048], P('fs', 'tp')
- output_copy: bfloat16 [1024, 2048], P(None, 'tp')
- output_first_new: float32 [128, 2048], P('fs', 'tp')
- output_second_new: float32 [128, 2048], P('fs', 'tp')
All inputs are finite; a program needn't handle non-finite values.
Results may differ from a plain program's by a relative error of at most 0.001.
Values may be sent and summed in bfloat16 or wider, within the bound.
No kernel may reach another device: no remote copies, remote signals or barrier semaphores. Data moves between devices by JAX's collectives and lax.ppermute only.
A program may use at most 64 MiB of HBM per device.

v0:
```python
import functools

import jax
import jax.numpy as jnp
from jax import lax
from jax.experimental import pallas as pl
from jax.experimental.pallas import tpu as pltpu
from jax.sharding import PartitionSpec as P


SMALL = pltpu.CompilerParams(vmem_limit_bytes=16 * 2**20)
highest = lax.Precision.HIGHEST
f32 = jnp.float32
bf16 = jnp.bfloat16
f16 = jnp.float16


def send_xor(x, axis, step):
    count = lax.axis_size(axis)
    return lax.ppermute(x, axis, [(i, i ^ step) for i in range(count)])


def finish_side(me, scale, projected, blocks, rows, factor, outs, direction, band):
    step_out, new_out, copy_out, first_out, second_out = outs
    for k, (first_old, second_old, _) in enumerate(blocks):
        at = pl.multiple_of((me ^ k) * band, band)
        scaled = scale * projected[pl.ds(at, band), :]
        first = 0.9 * first_old[...] + 0.1 * scaled
        second = 0.95 * second_old[...] + 0.05 * scaled * scaled
        if k == 0:
            first_out[...] = first
            second_out[...] = second
        direction[pl.ds(at, band), :] = first / (jnp.sqrt(second) + 1e-08)
    high = direction[...].astype(bf16)
    low = (direction[...] - high.astype(f32)).astype(bf16)
    for k, (_, _, master) in enumerate(blocks):
        at = pl.multiple_of((me ^ k) * rows, rows)
        own = factor[pl.ds(at, rows), :]
        step = jnp.dot(own, high, preferred_element_type=f32) + jnp.dot(
            own, low, preferred_element_type=f32
        )
        new = master[...] - 0.002 * step
        copy_out[pl.ds(at, rows), :] = new.astype(bf16)
        if k == 0:
            step_out[...] = step
            new_out[...] = new


def finish_kernel(chips, places, entries, value_rows, output_rows, *refs):
    tiles, refs = refs[:chips], refs[chips:]
    value_proj, output_proj, value_factor, output_factor = refs[:4]
    outs, direction = refs[-11:-1], refs[-1]
    packs = refs[4:-11]
    me = lax.axis_index("fs")
    sums = [t[0:1, :] for t in tiles]
    while len(sums) > 1:
        sums = [sums[2 * i] + sums[2 * i + 1] for i in range(len(sums) // 2)]
    scales = lax.rsqrt(sums[0] / entries + 1e-06)
    band = direction.shape[0] // len(places)
    value_blocks, output_blocks = [], []
    for (small, at), (large, at_large) in places:
        cuts = [packs[small].at[at + i * band : at + (i + 1) * band, :] for i in range(4)]
        value_master = packs[small].at[at + 4 * band : at + 4 * band + value_rows, :]
        output_master = packs[large].at[at_large : at_large + output_rows, :]
        value_blocks.append((cuts[0], cuts[1], value_master))
        output_blocks.append((cuts[2], cuts[3], output_master))
    for scale, projected, blocks, rows, factor, side_outs in (
        (scales[:, 0:1], value_proj, value_blocks, value_rows, value_factor, outs[:5]),
        (scales[:, 64:65], output_proj, output_blocks, output_rows, output_factor, outs[5:]),
    ):
        finish_side(me, scale, projected, blocks, rows, factor, side_outs, direction, band)


def finish(tiles, entries, value_proj, output_proj, value_factor, output_factor, smalls, larges):
    count = len(smalls)
    rank, columns = value_proj.shape
    band = rank // count
    value_rows, output_rows = value_factor.shape[0] // count, output_factor.shape[0] // count
    vmem = pl.BlockSpec(memory_space=pltpu.VMEM)
    arrays = []

    def place(part):
        array, at = part
        for i, known in enumerate(arrays):
            if known is array:
                return i, at
        arrays.append(array)
        return len(arrays) - 1, at

    places = tuple((place(small), place(large)) for small, large in zip(smalls, larges))

    def side(rows):
        return [
            jax.ShapeDtypeStruct((rows, columns), f32),
            jax.ShapeDtypeStruct((rows, columns), f32),
            jax.ShapeDtypeStruct((rows * count, columns), bf16),
            jax.ShapeDtypeStruct((band, columns), f32),
            jax.ShapeDtypeStruct((band, columns), f32),
        ]

    return pl.pallas_call(
        functools.partial(finish_kernel, len(tiles), places, entries, value_rows, output_rows),
        out_shape=side(value_rows) + side(output_rows),
        in_specs=[vmem] * (len(tiles) + 4 + len(arrays)),
        out_specs=[vmem] * 10,
        scratch_shapes=[pltpu.VMEM((rank, columns), f32)],
        compiler_params=SMALL,
        name="finish",
    )(*tiles, value_proj, output_proj, value_factor, output_factor, *arrays)


def term_kernel(x, out):
    rank, columns = x.shape
    root = jnp.maximum(jnp.sqrt(largest_of(x)) * 0.25, 2.0**-14)
    wide = root * (2.0**23 + 1.0)
    root = 2.0 * (wide - (wide - root))
    out[0:rank, :] = x[...] * (2048.0 / (root * root))
    out[rank : rank + 16, :] = jnp.broadcast_to(root, (16, columns))


def scaled_term(x):
    vmem = pl.BlockSpec(memory_space=pltpu.VMEM)
    rank, columns = x.shape
    return pl.pallas_call(
        term_kernel,
        out_shape=jax.ShapeDtypeStruct((rank + 16, columns), f32),
        in_specs=[vmem],
        out_specs=vmem,
        compiler_params=SMALL,
        cost_estimate=pl.CostEstimate(flops=100_000_000, bytes_accessed=0, transcendentals=0),
        name="scaled_term",
    )(x)


def square_kernel(value, output, squares):
    def square(x):
        return jnp.sum(jnp.sum(x * x, axis=0, keepdims=True), axis=1, keepdims=True)

    lane = lax.broadcasted_iota(jnp.int32, squares.shape, 1)
    squares[...] = jnp.where(lane < 64, square(value[...]), square(output[...]))


def sum_squares(value, output):
    vmem = pl.BlockSpec(memory_space=pltpu.VMEM)
    return pl.pallas_call(
        square_kernel,
        out_shape=jax.ShapeDtypeStruct((8, 128), f32),
        in_specs=[vmem] * 2,
        out_specs=vmem,
        compiler_params=SMALL,
        cost_estimate=pl.CostEstimate(flops=100_000_000, bytes_accessed=0, transcendentals=0),
        name="sum_squares",
    )(value, output)


def largest_of(x):
    return jnp.max(jnp.max(jnp.abs(x[...]).astype(f32), axis=0, keepdims=True), axis=1, keepdims=True)


def first_kernel(chips, heads, factor, parts, rows_out, factor_other):
    tokens, features = heads.shape
    half, rank = tokens // 2, factor.shape[1]
    chunk = half // chips
    place = lax.axis_index("tp")
    core, chip = place & 1, place >> 1
    own_factor = factor[pl.ds(pl.multiple_of(place * features, features), features), :]
    factor_other[...] = factor[pl.ds(pl.multiple_of((place ^ 1) * features, features), features), :]
    for k in range(chips):
        at = pl.multiple_of(core * half + (chip ^ k) * chunk, chunk)
        parts[k * chunk : (k + 1) * chunk, :] = jnp.dot(
            heads[pl.ds(at, chunk), :], own_factor, preferred_element_type=f32
        )
    largest = jnp.maximum(largest_of(heads), 2.0**-13)
    bound = jnp.maximum(largest_of(factor), 1e-30) * (2 * features / 32768.0)
    rows_out[0:8, :] = jnp.broadcast_to(largest, (8, rank))
    rows_out[8:16, :] = jnp.broadcast_to(bound, (8, rank))


def second_kernel(chips, heads, parts, rows, factor, *outs):
    tokens, _ = heads.shape
    half, rank = tokens // 2, factor.shape[1]
    chunk = half // chips
    place = lax.axis_index("tp")
    core, chip = place & 1, place >> 1
    largest = jnp.maximum(rows[0:1, :], largest_of(heads))
    bound = rows[8:9, :]
    scale = 1.0 / (bound * largest)
    other_factor = factor[...]
    for k in reversed(range(chips)):
        at = pl.multiple_of(core * half + (chip ^ k) * chunk, chunk)
        part = parts[k * chunk : (k + 1) * chunk, :] + jnp.dot(
            heads[pl.ds(at, chunk), :], other_factor, preferred_element_type=f32
        )
        if k == 0:
            outs[0][...] = part
        else:
            outs[k][0:chunk, :] = part * scale
            outs[k][chunk : chunk + 16, :] = jnp.broadcast_to(largest, (16, rank))
    outs[chips][0:8, :] = jnp.broadcast_to(largest, (8, rank))
    outs[chips][8:16, :] = jnp.broadcast_to(bound, (8, rank))


def partial_image(heads, heads_other, factor, chips):
    tokens, features = heads.shape
    rank = factor.shape[1]
    chunk = tokens // (2 * chips)
    vmem = pl.BlockSpec(memory_space=pltpu.VMEM)
    cost = pl.CostEstimate(flops=200_000_000, bytes_accessed=0, transcendentals=0)
    parts, rows, other_factor = pl.pallas_call(
        functools.partial(first_kernel, chips),
        out_shape=[
            jax.ShapeDtypeStruct((tokens // 2, rank), f32),
            jax.ShapeDtypeStruct((16, rank), f32),
            jax.ShapeDtypeStruct((features, rank), bf16),
        ],
        in_specs=[vmem] * 2,
        out_specs=[vmem] * 3,
        compiler_params=SMALL,
        cost_estimate=cost,
        name="partial_first",
    )(heads, factor)
    return pl.pallas_call(
        functools.partial(second_kernel, chips),
        out_shape=[jax.ShapeDtypeStruct((chunk, rank), f32)]
        + [jax.ShapeDtypeStruct((chunk + 16, rank), f32)] * (chips - 1)
        + [jax.ShapeDtypeStruct((16, rank), f32)],
        in_specs=[vmem] * 4,
        out_specs=[vmem] * (chips + 1),
        compiler_params=SMALL,
        cost_estimate=cost,
        name="partial_second",
    )(heads_other, parts, rows, other_factor)


def pack_kernel(*refs):
    *sources, packed = refs
    at = 0
    for x in sources:
        packed[at : at + x.shape[0], :] = x[...]
        at += x.shape[0]


def pack_rows(*arrays):
    rows = sum(x.shape[0] for x in arrays)
    vmem = pl.BlockSpec(memory_space=pltpu.VMEM)
    return pl.pallas_call(
        pack_kernel,
        out_shape=jax.ShapeDtypeStruct((rows, arrays[0].shape[1]), f32),
        in_specs=[vmem] * len(arrays),
        out_specs=vmem,
        compiler_params=SMALL,
        cost_estimate=pl.CostEstimate(flops=100_000_000, bytes_accessed=0, transcendentals=0),
        name="pack_rows",
    )(*arrays)


def add_kernel(a, b, out):
    out[...] = a[...] + b[...]


def add_tiles(a, b):
    vmem = pl.BlockSpec(memory_space=pltpu.VMEM)
    return pl.pallas_call(
        add_kernel,
        out_shape=jax.ShapeDtypeStruct(a.shape, f32),
        in_specs=[vmem] * 2,
        out_specs=vmem,
        compiler_params=SMALL,
        name="add_tiles",
    )(a, b)


def on_device(
    value_input,
    value_cotangent,
    value_factor,
    value_master,
    value_first,
    value_second,
    mixed_heads,
    output_cotangent,
    output_factor,
    output_master,
    output_first,
    output_second,
):
    fs_count = lax.axis_size("fs")
    tp_count = lax.axis_size("tp")
    tp_place = lax.axis_index("tp")
    chips = tp_count // 2
    core = tp_place & 1
    chip = tp_place >> 1
    rank = value_factor.shape[1]
    columns = value_input.shape[1]
    tokens, _ = mixed_heads.shape
    half = tokens // 2
    chunk = half // chips

    def project(image, cotangent):
        return lax.dot_general(
            image,
            cotangent.astype(f32),
            (((0,), (0,)), ((), ())),
            precision=highest,
            preferred_element_type=f32,
        )

    def sum_fs(term):
        own = scaled_term(term).astype(f16)
        terms = [own]
        for k in range(1, fs_count):
            terms.append(send_xor(own, "fs", k))
        sums = []
        for t in terms:
            root = t[rank : rank + 1].astype(f32)
            sums.append(t[:rank].astype(f32) * (root * root * 2.0**-11))
        while len(sums) > 1:
            sums = [sums[2 * i] + sums[2 * i + 1] for i in range(len(sums) // 2)]
        return sums[0]

    def gather_fs(packed, cut):
        if fs_count != 4:
            whole = [packed]
            for k in range(1, fs_count):
                whole.append(send_xor(packed, "fs", k))
            return [(w, 0) for w in whole], [(w, cut) for w in whole]
        near = send_xor(packed, "fs", 1)
        far = send_xor(packed, "fs", 2)
        first = send_xor(near[:cut], "fs", 2)
        last = send_xor(far[cut:], "fs", 1)
        parts = [packed, near, far]
        return [(p, 0) for p in parts] + [(first, 0)], [(p, cut) for p in parts] + [(last, 0)]

    heads_other = send_xor(mixed_heads, "tp", 1)

    value_image = jnp.dot(value_cotangent, value_factor, preferred_element_type=f32)
    value_term = project(value_image, value_input)

    total, *sends, scale_rows = partial_image(
        mixed_heads, heads_other, output_factor, chips
    )
    largest, bound = scale_rows[0:1], scale_rows[8:9]
    arrived = []
    for k in range(1, chips):
        arrived.append(send_xor(sends[k - 1].astype(f16), "tp", 2 * k))
    for a in arrived:
        of_peer = a[chunk : chunk + 1].astype(f32)
        largest = jnp.maximum(largest, of_peer)
        total += a[:chunk].astype(f32) * (bound * of_peer)
    bound_total = bound * (chips * largest)
    total = (total * (1.0 / bound_total)).astype(f16)

    products = []
    for k in range(chips):
        mine = send_xor(total, "tp", 2 * k) if k else total
        theirs = send_xor(mine, "tp", 1)
        for at, part in ((core * half, mine), ((1 - core) * half, theirs)):
            rows = lax.dynamic_slice_in_dim(output_cotangent, at + (chip ^ k) * chunk, chunk, 0)
            product = project(part.astype(f32), rows)
            products.append(product)
    output_term = sum(products[1:], products[0]) * bound_total[0, 0]

    value_proj = sum_fs(value_term)
    output_proj = sum_fs(output_term)

    small = (value_first, value_second, output_first, output_second, value_master)
    packed = pack_rows(*small, output_master)
    smalls, larges = gather_fs(packed, sum(x.shape[0] for x in small))

    squares = sum_squares(value_proj, output_proj)
    squares = add_tiles(squares, send_xor(squares, "tp", 1))
    tiles = [squares]
    for k in range(1, chips):
        tiles.append(send_xor(squares, "tp", 2 * k))
    return tuple(
        finish(
            tiles,
            1.0 * rank * columns * tp_count,
            value_proj,
            output_proj,
            value_factor,
            output_factor,
            smalls,
            larges,
        )
    )


def solution(mesh):
    in_specs = (
        P("fs", "tp"),
        P("fs", None),
        P(),
        P("fs", "tp"),
        P("fs", "tp"),
        P("fs", "tp"),
        P("fs", "tp"),
        P("fs", "tp"),
        P(),
        P("fs", "tp"),
        P("fs", "tp"),
        P("fs", "tp"),
    )
    out_specs = (
        P("fs", "tp"),
        P("fs", "tp"),
        P(None, "tp"),
        P("fs", "tp"),
        P("fs", "tp"),
        P("fs", "tp"),
        P("fs", "tp"),
        P(None, "tp"),
        P("fs", "tp"),
        P("fs", "tp"),
    )
    return jax.shard_map(
        on_device, mesh=mesh, in_specs=in_specs, out_specs=out_specs, check_vma=False
    )
```

profile of v0, /device:TPU:0, one launch (start us, length us, event | category | flops | bytes accessed | tf_op | source)
XLA Modules:
  0.0 69.1 jit_solution(2288506476664707993)
XLA Ops:
  0.7 1.1 %copy-done.3 = f32[256,256]{1,0:T(8,128)S(1)} copy-done((f32[256,256]{1,0:T(8,128)S(1)}, f32[256,256]{1,0:T(8,128)}, u32[]{:S(2)}) %copy-start.3) | copy-done | bytes 262168
  5.7 3.1 %collective-permute-start.22 = (f32[512,256]{1,0:T(8,128)S(1)}, f32[512,256]{1,0:T(8,128)S(1)}, u32[]{:S(2)}, u32[]{:S(2)}) collective-permute-start(f32[512,256]{1,0:T(8,128)S(1)} %pack_rows.1.refs_8_), channel_id=1, source_target_pairs={{0,16},{8,24},{16,0},{24,8},{1,17},{9,25},{17,1},{25,9},{2,18},{10... | collective-permute-start | bytes 1572872 | tf_op jit(solution)/shard_map/ppermute | solution.py:20
  8.8 1.5 %collective-permute-start.21 = (f32[512,256]{1,0:T(8,128)S(1)}, f32[512,256]{1,0:T(8,128)}, u32[]{:S(2)}, u32[]{:S(2)}) collective-permute-start(f32[512,256]{1,0:T(8,128)S(1)} %pack_rows.1.refs_8_), channel_id=1, source_target_pairs={{0,8},{8,0},{16,24},{24,16},{1,9},{9,1},{17,25},{25,17},{2,10},{10... | collective-permute-start | bytes 1572872 | tf_op jit(solution)/shard_map/ppermute | solution.py:20
  10.3 1.6 %fusion.38 = f32[2048,128]{1,0:T(8,128)S(1)} fusion(bf16[2048,512]{1,0:T(8,128)(2,1)S(1)} %copy-done, bf16[512,128]{1,0:T(8,128)(2,1)} %refs_6_.1), kind=kOutput, calls=%fused_computation.62 | convolution fusion | flops 268435456 | bytes 3276800 | tf_op jit(solution)/shard_map/dot_general | solution.py:336
  13.2 1.9 %collective-permute-start.1 = (f16[144,256]{1,0:T(8,128)(2,1)S(1)}, f16[144,256]{1,0:T(8,128)(2,1)}, u32[]{:S(2)}, u32[]{:S(2)}) collective-permute-start(f16[144,256]{1,0:T(8,128)(2,1)S(1)} %convert_element_type.101), channel_id=1, source_target_pairs={{0,16},{8,24},{16,0},{24,8},{1,17},{9,25},{17,1},{25,9},{2,18},{10... | collective-permute-start | bytes 221192 | tf_op jit(solution)/shard_map/ppermute | solution.py:20
  15.7 1.6 %partial_first.1 = (f32[1024,128]{1,0:T(8,128)S(1)}, f32[16,128]{1,0:T(8,128)S(1)}, bf16[128,128]{1,0:T(8,128)(2,1)S(1)}) custom-call(bf16[2048,128]{1,0:T(8,128)(2,1)} %heads.1, bf16[1024,128]{1,0:T(8,128)(2,1)S(1)} %copy-done.1), custom_call_target="tpu_custom_call" | custom-call | flops 200000000 | tf_op jit(solution)/shard_map/partial_first/pallas_call | solution.py:209
  17.3 6.3 %collective-permute-done.2 = f16[144,256]{1,0:T(8,128)(2,1)S(1)} collective-permute-done((f16[144,256]{1,0:T(8,128)(2,1)S(1)}, f16[144,256]{1,0:T(8,128)(2,1)S(1)}, u32[]{:S(2)}, u32[]{:S(2)}) %collective-permute-start.2) | collective-permute-done | bytes 73760 | tf_op jit(solution)/shard_map/ppermute | solution.py:20
  23.7 1.6 %collective-permute-start = (f16[144,256]{1,0:T(8,128)(2,1)S(1)}, f16[144,256]{1,0:T(8,128)(2,1)S(1)}, u32[]{:S(2)}, u32[]{:S(2)}) collective-permute-start(f16[144,256]{1,0:T(8,128)(2,1)S(1)} %convert_element_type.101), channel_id=1, source_target_pairs={{0,8},{8,0},{16,24},{24,16},{1,9},{9,1},{17,25},{25,17},{2,10},{10... | collective-permute-start | bytes 221192 | tf_op jit(solution)/shard_map/ppermute | solution.py:20
  26.0 2.0 %collective-permute-done = f16[144,256]{1,0:T(8,128)(2,1)S(1)} collective-permute-done((f16[144,256]{1,0:T(8,128)(2,1)S(1)}, f16[144,256]{1,0:T(8,128)(2,1)S(1)}, u32[]{:S(2)}, u32[]{:S(2)}) %collective-permute-start) | collective-permute-done | bytes 73760 | tf_op jit(solution)/shard_map/ppermute | solution.py:20
  28.0 1.5 %partial_second.1 = (f32[256,128]{1,0:T(8,128)S(1)}, f32[272,128]{1,0:T(8,128)S(1)}, f32[272,128]{1,0:T(8,128)S(1)}, f32[272,128]{1,0:T(8,128)S(1)}, f32[16,128]{1,0:T(8,128)S(1)}) custom-call(bf16[2048,128]{1,0:T(8,128)(2,1)} %collective-permute-done.3.heads, f32[1024,128]{1,0:T(8,128)S(1)} %get-tuple-element.18.parts, ...), custom_call_target="tpu_custom_call" | custom-call | flops 200000000 | tf_op jit(solution)/shard_map/partial_second/pallas_call | solution.py:222
  29.6 3.8 %collective-permute-start.6 = (f16[272,128]{1,0:T(8,128)(2,1)S(1)}, f16[272,128]{1,0:T(8,128)(2,1)S(1)}, u32[]{:S(2)}, u32[]{:S(2)}) collective-permute-start(f16[272,128]{1,0:T(8,128)(2,1)S(1)} %convert_element_type.116), channel_id=1, source_target_pairs={{0,6},{1,7},{2,4},{3,5},{4,2},{5,3},{6,0},{7,1},{8,14},{9,15},{10,... | collective-permute-start | bytes 208904 | tf_op jit(solution)/shard_map/ppermute | solution.py:20
  35.0 1.7 %collective-permute-start.24 = (f32[256,256]{1,0:T(8,128)S(1)}, f32[256,256]{1,0:T(8,128)S(1)}, u32[]{:S(2)}, u32[]{:S(2)}) collective-permute-start(f32[256,256]{1,0:T(8,128)S(1)} %slice.131), channel_id=1, source_target_pairs={{0,8},{8,0},{16,24},{24,16},{1,9},{9,1},{17,25},{25,17},{2,10},{10... | collective-permute-start | bytes 786440 | tf_op jit(solution)/shard_map/ppermute | solution.py:20
  37.7 1.6 %collective-permute-start.23 = (f32[256,256]{1,0:T(8,128)S(1)}, f32[256,256]{1,0:T(8,128)S(1)}, u32[]{:S(2)}, u32[]{:S(2)}) collective-permute-start(f32[256,256]{1,0:T(8,128)S(1)} %slice.130), channel_id=1, source_target_pairs={{0,16},{8,24},{16,0},{24,8},{1,17},{9,25},{17,1},{25,9},{2,18},{10... | collective-permute-start | bytes 786440 | tf_op jit(solution)/shard_map/ppermute | solution.py:20
  39.4 3.7 %collective-permute-start.12 = (f16[256,128]{1,0:T(8,128)(2,1)S(1)}, f16[256,128]{1,0:T(8,128)(2,1)S(1)}, u32[]{:S(2)}, u32[]{:S(2)}) collective-permute-start(f16[256,128]{1,0:T(8,128)(2,1)S(1)} %multiply_convert_fusion), channel_id=1, source_target_pairs={{0,6},{1,7},{2,4},{3,5},{4,2},{5,3},{6,0},{7,1},{8,14},{9,15},{10,... | collective-permute-start | bytes 196616 | tf_op jit(solution)/shard_map/ppermute | solution.py:20
  44.1 4.1 %collective-permute-done.10 = f16[256,128]{1,0:T(8,128)(2,1)S(1)} collective-permute-done((f16[256,128]{1,0:T(8,128)(2,1)S(1)}, f16[256,128]{1,0:T(8,128)(2,1)S(1)}, u32[]{:S(2)}, u32[]{:S(2)}) %collective-permute-start.10) | collective-permute-done | bytes 65568 | tf_op jit(solution)/shard_map/ppermute | solution.py:20
  51.7 1.8 %collective-permute-start.16 = (f16[144,256]{1,0:T(8,128)(2,1)S(1)}, f16[144,256]{1,0:T(8,128)(2,1)S(1)}, u32[]{:S(2)}, u32[]{:S(2)}) collective-permute-start(f16[144,256]{1,0:T(8,128)(2,1)S(1)} %convert_element_type.120), channel_id=1, source_target_pairs={{0,24},{8,16},{16,8},{24,0},{1,25},{9,17},{17,9},{25,1},{2,26},{10... | collective-permute-start | bytes 221192 | tf_op jit(solution)/shard_map/ppermute | solution.py:20
  54.0 1.3 %collective-permute-start.14 = (f16[144,256]{1,0:T(8,128)(2,1)S(1)}, f16[144,256]{1,0:T(8,128)(2,1)S(1)}, u32[]{:S(2)}, u32[]{:S(2)}) collective-permute-start(f16[144,256]{1,0:T(8,128)(2,1)S(1)} %convert_element_type.120), channel_id=1, source_target_pairs={{0,8},{8,0},{16,24},{24,16},{1,9},{9,1},{17,25},{25,17},{2,10},{10... | collective-permute-start | bytes 221192 | tf_op jit(solution)/shard_map/ppermute | solution.py:20
  55.2 1.8 %collective-permute-done.16 = f16[144,256]{1,0:T(8,128)(2,1)S(1)} collective-permute-done((f16[144,256]{1,0:T(8,128)(2,1)S(1)}, f16[144,256]{1,0:T(8,128)(2,1)S(1)}, u32[]{:S(2)}, u32[]{:S(2)}) %collective-permute-start.16) | collective-permute-done | bytes 73760 | tf_op jit(solution)/shard_map/ppermute | solution.py:20
  57.1 1.5 %collective-permute-done.15 = f16[144,256]{1,0:T(8,128)(2,1)S(1)} collective-permute-done((f16[144,256]{1,0:T(8,128)(2,1)S(1)}, f16[144,256]{1,0:T(8,128)(2,1)S(1)}, u32[]{:S(2)}, u32[]{:S(2)}) %collective-permute-start.15) | collective-permute-done | bytes 73760 | tf_op jit(solution)/shard_map/ppermute | solution.py:20
  58.8 1.1 %collective-permute-done.17.b = f32[8,128]{1,0:T(8,128)S(1)} collective-permute-done((f32[8,128]{1,0:T(8,128)S(1)}, f32[8,128]{1,0:T(8,128)S(1)}, u32[]{:S(2)}, u32[]{:S(2)}) %collective-permute-start.17) | collective-permute-done | bytes 4128 | tf_op jit(solution)/shard_map/ppermute | solution.py:20
  59.9 1.8 %collective-permute-start.20 = (f32[8,128]{1,0:T(8,128)S(1)}, f32[8,128]{1,0:T(8,128)S(1)}, u32[]{:S(2)}, u32[]{:S(2)}) collective-permute-start(f32[8,128]{1,0:T(8,128)S(1)} %add_tiles.1.refs_0_), channel_id=1, source_target_pairs={{0,6},{1,7},{2,4},{3,5},{4,2},{5,3},{6,0},{7,1},{8,14},{9,15},{10,... | collective-permute-start | bytes 12296 | tf_op jit(solution)/shard_map/ppermute | solution.py:20
  61.8 2.5 %collective-permute-start.18 = (f32[8,128]{1,0:T(8,128)S(1)}, f32[8,128]{1,0:T(8,128)S(1)}, u32[]{:S(2)}, u32[]{:S(2)}) collective-permute-start(f32[8,128]{1,0:T(8,128)S(1)} %add_tiles.1.refs_0_), channel_id=1, source_target_pairs={{0,2},{1,3},{2,0},{3,1},{4,6},{5,7},{6,4},{7,5},{8,10},{9,11},{10,... | collective-permute-start | bytes 12296 | tf_op jit(solution)/shard_map/ppermute | solution.py:20
  64.3 1.0 %collective-permute-done.20.refs_3_ = f32[8,128]{1,0:T(8,128)S(1)} collective-permute-done((f32[8,128]{1,0:T(8,128)S(1)}, f32[8,128]{1,0:T(8,128)S(1)}, u32[]{:S(2)}, u32[]{:S(2)}) %collective-permute-start.20) | collective-permute-done | bytes 4128 | tf_op jit(solution)/shard_map/ppermute | solution.py:20
  66.3 2.8 %finish.1 = (f32[128,256]{1,0:T(8,128)}, f32[128,256]{1,0:T(8,128)}, bf16[512,256]{1,0:T(8,128)(2,1)}, f32[32,256]{1,0:T(8,128)}, f32[32,256]{1,0:T(8,128)}, /*i...) custom-call(f32[8,128]{1,0:T(8,128)S(1)} %add_tiles.1.refs_0_, ...), custom_call_target="tpu_custom_call" | custom-call | tf_op jit(solution)/shard_map/finish/pallas_call | solution.py:101
  (87 shorter events, 15.3 us)
Async XLA Ops:
  5.7 29.2 %collective-permute-start.22 = (f32[512,256]{1,0:T(8,128)S(1)}, f32[512,256]{1,0:T(8,128)S(1)}, u32[]{:S(2)}, u32[]{:S(2)}) collective-permute-start(f32[512,256]{1,0:T(8,128)S(1)} %pack_rows.1.refs_8_), channel_id=1, source_target_pairs={{0,16},{8,24},{16,0},{24,8},{1,17},{9,25},{17,1},{25,9},{2,18},{10... | collective-permute-start | bytes 1572872 | tf_op jit(solution)/shard_map/ppermute | solution.py:20
  8.8 27.9 %collective-permute-start.21 = (f32[512,256]{1,0:T(8,128)S(1)}, f32[512,256]{1,0:T(8,128)}, u32[]{:S(2)}, u32[]{:S(2)}) collective-permute-start(f32[512,256]{1,0:T(8,128)S(1)} %pack_rows.1.refs_8_), channel_id=1, source_target_pairs={{0,8},{8,0},{16,24},{24,16},{1,9},{9,1},{17,25},{25,17},{2,10},{10... | collective-permute-start | bytes 1572872 | tf_op jit(solution)/shard_map/ppermute | solution.py:20
  13.1 10.6 %collective-permute-start.2 = (f16[144,256]{1,0:T(8,128)(2,1)S(1)}, f16[144,256]{1,0:T(8,128)(2,1)S(1)}, u32[]{:S(2)}, u32[]{:S(2)}) collective-permute-start(f16[144,256]{1,0:T(8,128)(2,1)S(1)} %convert_element_type.101), channel_id=1, source_target_pairs={{0,24},{8,16},{16,8},{24,0},{1,25},{9,17},{17,9},{25,1},{2,26},{10... | collective-permute-start | bytes 221192 | tf_op jit(solution)/shard_map/ppermute | solution.py:20
  13.2 12.1 %collective-permute-start.1 = (f16[144,256]{1,0:T(8,128)(2,1)S(1)}, f16[144,256]{1,0:T(8,128)(2,1)}, u32[]{:S(2)}, u32[]{:S(2)}) collective-permute-start(f16[144,256]{1,0:T(8,128)(2,1)S(1)} %convert_element_type.101), channel_id=1, source_target_pairs={{0,16},{8,24},{16,0},{24,8},{1,17},{9,25},{17,1},{25,9},{2,18},{10... | collective-permute-start | bytes 221192 | tf_op jit(solution)/shard_map/ppermute | solution.py:20
  15.1 12.9 %collective-permute-start.3 = (bf16[2048,128]{1,0:T(8,128)(2,1)}, bf16[2048,128]{1,0:T(8,128)(2,1)}, u32[]{:S(2)}, u32[]{:S(2)}) collective-permute-start(bf16[2048,128]{1,0:T(8,128)(2,1)} %heads.1), channel_id=1, source_target_pairs={{0,1},{1,0},{2,3},{3,2},{4,5},{5,4},{6,7},{7,6},{8,9},{9,8},{10,11... | collective-permute-start | bytes 1572872 | tf_op jit(solution)/shard_map/ppermute | solution.py:20
  23.7 4.4 %collective-permute-start = (f16[144,256]{1,0:T(8,128)(2,1)S(1)}, f16[144,256]{1,0:T(8,128)(2,1)S(1)}, u32[]{:S(2)}, u32[]{:S(2)}) collective-permute-start(f16[144,256]{1,0:T(8,128)(2,1)S(1)} %convert_element_type.101), channel_id=1, source_target_pairs={{0,8},{8,0},{16,24},{24,16},{1,9},{9,1},{17,25},{25,17},{2,10},{10... | collective-permute-start | bytes 221192 | tf_op jit(solution)/shard_map/ppermute | solution.py:20
  29.6 9.7 %collective-permute-start.6 = (f16[272,128]{1,0:T(8,128)(2,1)S(1)}, f16[272,128]{1,0:T(8,128)(2,1)S(1)}, u32[]{:S(2)}, u32[]{:S(2)}) collective-permute-start(f16[272,128]{1,0:T(8,128)(2,1)S(1)} %convert_element_type.116), channel_id=1, source_target_pairs={{0,6},{1,7},{2,4},{3,5},{4,2},{5,3},{6,0},{7,1},{8,14},{9,15},{10,... | collective-permute-start | bytes 208904 | tf_op jit(solution)/shard_map/ppermute | solution.py:20
  33.4 5.8 %collective-permute-start.5 = (f16[272,128]{1,0:T(8,128)(2,1)S(1)}, f16[272,128]{1,0:T(8,128)(2,1)S(1)}, u32[]{:S(2)}, u32[]{:S(2)}) collective-permute-start(f16[272,128]{1,0:T(8,128)(2,1)S(1)} %convert_element_type.113), channel_id=1, source_target_pairs={{0,4},{1,5},{2,6},{3,7},{4,0},{5,1},{6,2},{7,3},{8,12},{9,13},{10,... | collective-permute-start | bytes 208904 | tf_op jit(solution)/shard_map/ppermute | solution.py:20
  33.4 5.8 %collective-permute-start.4 = (f16[272,128]{1,0:T(8,128)(2,1)S(1)}, f16[272,128]{1,0:T(8,128)(2,1)S(1)}, u32[]{:S(2)}, u32[]{:S(2)}) collective-permute-start(f16[272,128]{1,0:T(8,128)(2,1)S(1)} %convert_element_type.110), channel_id=1, source_target_pairs={{0,2},{1,3},{2,0},{3,1},{4,6},{5,7},{6,4},{7,5},{8,10},{9,11},{10,... | collective-permute-start | bytes 208904 | tf_op jit(solution)/shard_map/ppermute | solution.py:20
  35.0 29.3 %collective-permute-start.24 = (f32[256,256]{1,0:T(8,128)S(1)}, f32[256,256]{1,0:T(8,128)S(1)}, u32[]{:S(2)}, u32[]{:S(2)}) collective-permute-start(f32[256,256]{1,0:T(8,128)S(1)} %slice.131), channel_id=1, source_target_pairs={{0,8},{8,0},{16,24},{24,16},{1,9},{9,1},{17,25},{25,17},{2,10},{10... | collective-permute-start | bytes 786440 | tf_op jit(solution)/shard_map/ppermute | solution.py:20
  37.7 26.6 %collective-permute-start.23 = (f32[256,256]{1,0:T(8,128)S(1)}, f32[256,256]{1,0:T(8,128)S(1)}, u32[]{:S(2)}, u32[]{:S(2)}) collective-permute-start(f32[256,256]{1,0:T(8,128)S(1)} %slice.130), channel_id=1, source_target_pairs={{0,16},{8,24},{16,0},{24,8},{1,17},{9,25},{17,1},{25,9},{2,18},{10... | collective-permute-start | bytes 786440 | tf_op jit(solution)/shard_map/ppermute | solution.py:20
  39.4 9.1 %collective-permute-start.12 = (f16[256,128]{1,0:T(8,128)(2,1)S(1)}, f16[256,128]{1,0:T(8,128)(2,1)S(1)}, u32[]{:S(2)}, u32[]{:S(2)}) collective-permute-start(f16[256,128]{1,0:T(8,128)(2,1)S(1)} %multiply_convert_fusion), channel_id=1, source_target_pairs={{0,6},{1,7},{2,4},{3,5},{4,2},{5,3},{6,0},{7,1},{8,14},{9,15},{10,... | collective-permute-start | bytes 196616 | tf_op jit(solution)/shard_map/ppermute | solution.py:20
  43.0 5.2 %collective-permute-start.10 = (f16[256,128]{1,0:T(8,128)(2,1)S(1)}, f16[256,128]{1,0:T(8,128)(2,1)S(1)}, u32[]{:S(2)}, u32[]{:S(2)}) collective-permute-start(f16[256,128]{1,0:T(8,128)(2,1)S(1)} %multiply_convert_fusion), channel_id=1, source_target_pairs={{0,4},{1,5},{2,6},{3,7},{4,0},{5,1},{6,2},{7,3},{8,12},{9,13},{10,... | collective-permute-start | bytes 196616 | tf_op jit(solution)/shard_map/ppermute | solution.py:20
  43.0 6.0 %collective-permute-start.8 = (f16[256,128]{1,0:T(8,128)(2,1)S(1)}, f16[256,128]{1,0:T(8,128)(2,1)S(1)}, u32[]{:S(2)}, u32[]{:S(2)}) collective-permute-start(f16[256,128]{1,0:T(8,128)(2,1)S(1)} %multiply_convert_fusion), channel_id=1, source_target_pairs={{0,2},{1,3},{2,0},{3,1},{4,6},{5,7},{6,4},{7,5},{8,10},{9,11},{10,... | collective-permute-start | bytes 196616 | tf_op jit(solution)/shard_map/ppermute | solution.py:20
  48.2 1.3 %collective-permute-start.7 = (f16[256,128]{1,0:T(8,128)(2,1)S(1)}, f16[256,128]{1,0:T(8,128)(2,1)S(1)}, u32[]{:S(2)}, u32[]{:S(2)}) collective-permute-start(f16[256,128]{1,0:T(8,128)(2,1)S(1)} %multiply_convert_fusion), channel_id=1, source_target_pairs={{0,1},{1,0},{2,3},{3,2},{4,5},{5,4},{6,7},{7,6},{8,9},{9,8},{10,11... | collective-permute-start | bytes 196616 | tf_op jit(solution)/shard_map/ppermute | solution.py:20
  48.5 2.5 %collective-permute-start.11 = (f16[256,128]{1,0:T(8,128)(2,1)S(1)}, f16[256,128]{1,0:T(8,128)(2,1)S(1)}, u32[]{:S(2)}, u32[]{:S(2)}) collective-permute-start(f16[256,128]{1,0:T(8,128)(2,1)S(1)} %collective-permute-done.10), channel_id=1, source_target_pairs={{0,1},{1,0},{2,3},{3,2},{4,5},{5,4},{6,7},{7,6},{8,9},{9,8},{10,11... | collective-permute-start | bytes 196616 | tf_op jit(solution)/shard_map/ppermute | solution.py:20
  49.0 2.2 %collective-permute-start.13 = (f16[256,128]{1,0:T(8,128)(2,1)S(1)}, f16[256,128]{1,0:T(8,128)(2,1)S(1)}, u32[]{:S(2)}, u32[]{:S(2)}) collective-permute-start(f16[256,128]{1,0:T(8,128)(2,1)S(1)} %collective-permute-done.12), channel_id=1, source_target_pairs={{0,1},{1,0},{2,3},{3,2},{4,5},{5,4},{6,7},{7,6},{8,9},{9,8},{10,11... | collective-permute-start | bytes 196616 | tf_op jit(solution)/shard_map/ppermute | solution.py:20
  49.4 1.3 %collective-permute-start.9 = (f16[256,128]{1,0:T(8,128)(2,1)S(1)}, f16[256,128]{1,0:T(8,128)(2,1)S(1)}, u32[]{:S(2)}, u32[]{:S(2)}) collective-permute-start(f16[256,128]{1,0:T(8,128)(2,1)S(1)} %collective-permute-done.8), channel_id=1, source_target_pairs={{0,1},{1,0},{2,3},{3,2},{4,5},{5,4},{6,7},{7,6},{8,9},{9,8},{10,11... | collective-permute-start | bytes 196616 | tf_op jit(solution)/shard_map/ppermute | solution.py:20
  51.7 5.4 %collective-permute-start.16 = (f16[144,256]{1,0:T(8,128)(2,1)S(1)}, f16[144,256]{1,0:T(8,128)(2,1)S(1)}, u32[]{:S(2)}, u32[]{:S(2)}) collective-permute-start(f16[144,256]{1,0:T(8,128)(2,1)S(1)} %convert_element_type.120), channel_id=1, source_target_pairs={{0,24},{8,16},{16,8},{24,0},{1,25},{9,17},{17,9},{25,1},{2,26},{10... | collective-permute-start | bytes 221192 | tf_op jit(solution)/shard_map/ppermute | solution.py:20
  53.5 5.1 %collective-permute-start.15 = (f16[144,256]{1,0:T(8,128)(2,1)S(1)}, f16[144,256]{1,0:T(8,128)(2,1)S(1)}, u32[]{:S(2)}, u32[]{:S(2)}) collective-permute-start(f16[144,256]{1,0:T(8,128)(2,1)S(1)} %convert_element_type.120), channel_id=1, source_target_pairs={{0,16},{8,24},{16,0},{24,8},{1,17},{9,25},{17,1},{25,9},{2,18},{10... | collective-permute-start | bytes 221192 | tf_op jit(solution)/shard_map/ppermute | solution.py:20
  54.0 4.6 %collective-permute-start.14 = (f16[144,256]{1,0:T(8,128)(2,1)S(1)}, f16[144,256]{1,0:T(8,128)(2,1)S(1)}, u32[]{:S(2)}, u32[]{:S(2)}) collective-permute-start(f16[144,256]{1,0:T(8,128)(2,1)S(1)} %convert_element_type.120), channel_id=1, source_target_pairs={{0,8},{8,0},{16,24},{24,16},{1,9},{9,1},{17,25},{25,17},{2,10},{10... | collective-permute-start | bytes 221192 | tf_op jit(solution)/shard_map/ppermute | solution.py:20
  59.9 5.4 %collective-permute-start.20 = (f32[8,128]{1,0:T(8,128)S(1)}, f32[8,128]{1,0:T(8,128)S(1)}, u32[]{:S(2)}, u32[]{:S(2)}) collective-permute-start(f32[8,128]{1,0:T(8,128)S(1)} %add_tiles.1.refs_0_), channel_id=1, source_target_pairs={{0,6},{1,7},{2,4},{3,5},{4,2},{5,3},{6,0},{7,1},{8,14},{9,15},{10,... | collective-permute-start | bytes 12296 | tf_op jit(solution)/shard_map/ppermute | solution.py:20
  61.8 4.5 %collective-permute-start.19 = (f32[8,128]{1,0:T(8,128)S(1)}, f32[8,128]{1,0:T(8,128)S(1)}, u32[]{:S(2)}, u32[]{:S(2)}) collective-permute-start(f32[8,128]{1,0:T(8,128)S(1)} %add_tiles.1.refs_0_), channel_id=1, source_target_pairs={{0,4},{1,5},{2,6},{3,7},{4,0},{5,1},{6,2},{7,3},{8,12},{9,13},{10,... | collective-permute-start | bytes 12296 | tf_op jit(solution)/shard_map/ppermute | solution.py:20
  61.8 4.5 %collective-permute-start.18 = (f32[8,128]{1,0:T(8,128)S(1)}, f32[8,128]{1,0:T(8,128)S(1)}, u32[]{:S(2)}, u32[]{:S(2)}) collective-permute-start(f32[8,128]{1,0:T(8,128)S(1)} %add_tiles.1.refs_0_), channel_id=1, source_target_pairs={{0,2},{1,3},{2,0},{3,1},{4,6},{5,7},{6,4},{7,5},{8,10},{9,11},{10,... | collective-permute-start | bytes 12296 | tf_op jit(solution)/shard_map/ppermute | solution.py:20
  (13 other events, 90.1 us)
where the time goes:
time: 69.8 us; the launch traced here: 69.1 us
  starting transfers between devices  29.2 us (42%)
  waiting for transfers between devices  19.6 us (28%)
  Pallas kernels  6.3 us (9%)
  local copies, waits for them, and re-layouts  6.04 us (9%)
  matrix products  4.63 us (7%)
  other arithmetic  2.37 us (3%)
  between operations  0.93 us (1%)
    ppermute x25, starting transfers between devices, send_xor(): return lax.ppermute(x, axis, [(i, i ^ step) for i in range(count)])  29.2 us
    ppermute x25, waiting for transfers between devices, send_xor(): return lax.ppermute(x, axis, [(i, i ^ step) for i in range(count)])  19.6 us
    unnamed x24, local copies, waits for them, and re-layouts  5.06 us
    dot_general x9, matrix products, project(): lax.dot_general(image, cotangent.astype(f32), (((0,), (0,)), ((), ())), p...  3.04 us
    pallas_call x1, Pallas kernels, finish(): pl.pallas_call(functools.partial(finish_kernel, len(tiles), places, entri...  2.81 us
    dot_general x1, matrix products, on_device(): jnp.dot(value_cotangent, value_factor, preferred_element_type=f32)  1.6 us
    pallas_call x1, Pallas kernels, partial_image(): pl.pallas_call(functools.partial(first_kernel, chips), out_shape=[jax.Sha...  1.59 us
    pallas_call x1, Pallas kernels, partial_image(): pl.pallas_call(functools.partial(second_kernel, chips), out_shape=[jax.Sh...  1.51 us
  transfers between devices with their start and end apart: 25, of which 10 were waited for; matrix products, arithmetic and copies ran while one was open for 12% of the time, Pallas kernels for 5%

commit v1 on v0

--- a/solution.py
+++ b/solution.py
@@ -9,7 +9,7 @@
 
 
 SMALL = pltpu.CompilerParams(vmem_limit_bytes=16 * 2**20)
-highest = lax.Precision.HIGHEST
+highest = lax.Precision.HIGH
 f32 = jnp.float32
 bf16 = jnp.bfloat16
 f16 = jnp.float16
@@ -18,6 +18,10 @@
 def send_xor(x, axis, step):
     count = lax.axis_size(axis)
     return lax.ppermute(x, axis, [(i, i ^ step) for i in range(count)])
+
+
+def send_split(x):
+    return lax.ppermute(x, "tp", [(i, i ^ (6 if i & 1 else 2)) for i in range(8)])
 
 
 def finish_side(me, scale, projected, blocks, rows, factor, outs, direction, band):
@@ -157,35 +161,34 @@
     return jnp.max(jnp.max(jnp.abs(x[...]).astype(f32), axis=0, keepdims=True), axis=1, keepdims=True)
 
 
-def first_kernel(chips, heads, factor, parts, rows_out, factor_other):
+def first_kernel(chips, heads, factor, parts, rows_out):
     tokens, features = heads.shape
     half, rank = tokens // 2, factor.shape[1]
     chunk = half // chips
     place = lax.axis_index("tp")
     core, chip = place & 1, place >> 1
-    own_factor = factor[pl.ds(pl.multiple_of(place * features, features), features), :]
-    factor_other[...] = factor[pl.ds(pl.multiple_of((place ^ 1) * features, features), features), :]
+    own_factor = factor[pl.ds(pl.multiple_of(core * features, features), features), :]
     for k in range(chips):
         at = pl.multiple_of(core * half + (chip ^ k) * chunk, chunk)
         parts[k * chunk : (k + 1) * chunk, :] = jnp.dot(
             heads[pl.ds(at, chunk), :], own_factor, preferred_element_type=f32
         )
-    largest = jnp.maximum(largest_of(heads), 2.0**-13)
-    bound = jnp.maximum(largest_of(factor), 1e-30) * (2 * features / 32768.0)
-    rows_out[0:8, :] = jnp.broadcast_to(largest, (8, rank))
-    rows_out[8:16, :] = jnp.broadcast_to(bound, (8, rank))
+    rows_out[0:8, :] = jnp.broadcast_to(jnp.maximum(largest_of(heads), 2.0**-13), (8, rank))
+    rows_out[8:16, :] = jnp.broadcast_to(jnp.maximum(largest_of(factor), 2.0**-13), (8, rank))
 
 
 def second_kernel(chips, heads, parts, rows, factor, *outs):
-    tokens, _ = heads.shape
+    tokens, features = heads.shape
     half, rank = tokens // 2, factor.shape[1]
     chunk = half // chips
     place = lax.axis_index("tp")
     core, chip = place & 1, place >> 1
     largest = jnp.maximum(rows[0:1, :], largest_of(heads))
-    bound = rows[8:9, :]
-    scale = 1.0 / (bound * largest)
-    other_factor = factor[...]
+    marks = jnp.concatenate(
+        [jnp.broadcast_to(largest, (8, rank)), jnp.broadcast_to(rows[8:9, :], (8, rank))], axis=0
+    )
+    scale = 1.0 / (largest * rows[8:9, :] * term_bound(features))
+    other_factor = factor[pl.ds(pl.multiple_of((core ^ 1) * features, features), features), :]
     for k in reversed(range(chips)):
         at = pl.multiple_of(core * half + (chip ^ k) * chunk, chunk)
         part = parts[k * chunk : (k + 1) * chunk, :] + jnp.dot(
@@ -195,26 +198,28 @@
             outs[0][...] = part
         else:
             outs[k][0:chunk, :] = part * scale
-            outs[k][chunk : chunk + 16, :] = jnp.broadcast_to(largest, (16, rank))
-    outs[chips][0:8, :] = jnp.broadcast_to(largest, (8, rank))
-    outs[chips][8:16, :] = jnp.broadcast_to(bound, (8, rank))
+            outs[k][chunk : chunk + 16, :] = marks
+    outs[chips][...] = marks
+
+
+def term_bound(features):
+    return 2 * features / 32768.0
 
 
 def partial_image(heads, heads_other, factor, chips):
-    tokens, features = heads.shape
+    tokens, _ = heads.shape
     rank = factor.shape[1]
     chunk = tokens // (2 * chips)
     vmem = pl.BlockSpec(memory_space=pltpu.VMEM)
     cost = pl.CostEstimate(flops=200_000_000, bytes_accessed=0, transcendentals=0)
-    parts, rows, other_factor = pl.pallas_call(
+    parts, rows = pl.pallas_call(
         functools.partial(first_kernel, chips),
         out_shape=[
             jax.ShapeDtypeStruct((tokens // 2, rank), f32),
             jax.ShapeDtypeStruct((16, rank), f32),
-            jax.ShapeDtypeStruct((features, rank), bf16),
         ],
         in_specs=[vmem] * 2,
-        out_specs=[vmem] * 3,
+        out_specs=[vmem] * 2,
         compiler_params=SMALL,
         cost_estimate=cost,
         name="partial_first",
@@ -229,7 +234,7 @@
         compiler_params=SMALL,
         cost_estimate=cost,
         name="partial_second",
-    )(heads_other, parts, rows, other_factor)
+    )(heads_other, parts, rows, factor)
 
 
 def pack_kernel(*refs):
@@ -292,7 +297,7 @@
     chip = tp_place >> 1
     rank = value_factor.shape[1]
     columns = value_input.shape[1]
-    tokens, _ = mixed_heads.shape
+    tokens, features = mixed_heads.shape
     half = tokens // 2
     chunk = half // chips
 
@@ -337,17 +342,20 @@
     value_term = project(value_image, value_input)
 
     total, *sends, scale_rows = partial_image(
-        mixed_heads, heads_other, output_factor, chips
-    )
-    largest, bound = scale_rows[0:1], scale_rows[8:9]
+        mixed_heads,
+        heads_other,
+        lax.dynamic_slice_in_dim(output_factor, chip * (2 * features), 2 * features, 0),
+        chips,
+    )
+    strength = scale_rows[0:1] * scale_rows[8:9]
     arrived = []
     for k in range(1, chips):
         arrived.append(send_xor(sends[k - 1].astype(f16), "tp", 2 * k))
     for a in arrived:
-        of_peer = a[chunk : chunk + 1].astype(f32)
-        largest = jnp.maximum(largest, of_peer)
-        total += a[:chunk].astype(f32) * (bound * of_peer)
-    bound_total = bound * (chips * largest)
+        of_peer = a[chunk : chunk + 1].astype(f32) * a[chunk + 8 : chunk + 9].astype(f32)
+        strength = jnp.maximum(strength, of_peer)
+        total += a[:chunk].astype(f32) * (term_bound(features) * of_peer)
+    bound_total = chips * term_bound(features) * strength
     total = (total * (1.0 / bound_total)).astype(f16)
 
     products = []
@@ -370,8 +378,13 @@
     squares = sum_squares(value_proj, output_proj)
     squares = add_tiles(squares, send_xor(squares, "tp", 1))
     tiles = [squares]
-    for k in range(1, chips):
-        tiles.append(send_xor(squares, "tp", 2 * k))
+    if chips == 4:
+        tiles.append(send_split(squares))
+        tiles.append(send_xor(squares, "tp", 4))
+        tiles.append(send_xor(tiles[1], "tp", 1))
+    else:
+        for k in range(1, chips):
+            tiles.append(send_xor(squares, "tp", 2 * k))
     return tuple(
         finish(
             tiles,

time: 69.8 us -> 68.8 us (0.986)
  starting transfers between devices: 29.2 us -> 28.1 us
    ppermute x0 -> x1, waiting for transfers between devices: none -> 1.21 us  [send_split(): lax.ppermute(x, 'tp', [(i, i ^ (6 if i & 1 else 2)) for i in range(8)])]
    ppermute x25 -> x24, starting transfers between devices: 29.2 us -> 28.1 us  [send_xor(): return lax.ppermute(x, axis, [(i, i ^ step) for i in range(count)])]
    ppermute x25 -> x24, waiting for transfers between devices: 19.6 us -> 18.7 us  [send_xor(): return lax.ppermute(x, axis, [(i, i ^ step) for i in range(count)])]
    unnamed x24 -> x22, local copies, waits for them, and re-layouts: 5.06 us -> 5.06 us
  transfers between devices with their start and end apart: 25 -> 25, of which waited for: 10 -> 11; matrix products, arithmetic and copies ran while one was open for 12% -> 12% of each run, Pallas kernels for 5% -> 5%
where the time goes in v1:
time: 68.8 us; the launch traced here: 68.1 us
  starting transfers between devices  28.1 us (41%)
  waiting for transfers between devices  19.9 us (29%)
  Pallas kernels  6.25 us (9%)
  local copies, waits for them, and re-layouts  6.05 us (9%)
  matrix products  4.36 us (6%)
  other arithmetic  2.51 us (4%)
  between operations  1 us (1%)
    ppermute x24, starting transfers between devices, send_xor(): return lax.ppermute(x, axis, [(i, i ^ step) for i in range(count)])  28.1 us
    ppermute x24, waiting for transfers between devices, send_xor(): return lax.ppermute(x, axis, [(i, i ^ step) for i in range(count)])  18.7 us
    unnamed x22, local copies, waits for them, and re-layouts  5.06 us
    pallas_call x1, Pallas kernels, finish(): pl.pallas_call(functools.partial(finish_kernel, len(tiles), places, entri...  2.81 us
    dot_general x9, matrix products, project(): lax.dot_general(image, cotangent.astype(f32), (((0,), (0,)), ((), ())), p...  2.76 us
    dot_general x1, matrix products, on_device(): jnp.dot(value_cotangent, value_factor, preferred_element_type=f32)  1.6 us
    pallas_call x1, Pallas kernels, partial_image(): pl.pallas_call(functools.partial(first_kernel, chips), out_shape=[jax.Sha...  1.56 us
    pallas_call x1, Pallas kernels, partial_image(): pl.pallas_call(functools.partial(second_kernel, chips), out_shape=[jax.Sh...  1.51 us
  transfers between devices with their start and end apart: 25, of which 11 were waited for; matrix products, arithmetic and copies ran while one was open for 12% of the time, Pallas kernels for 5%

profile of v1, /device:TPU:0, one launch (start us, length us, event | category | flops | bytes accessed | tf_op | source)
XLA Modules:
  0.0 68.1 jit_solution(3604676917628837435)
XLA Ops:
  0.7 1.1 %copy-done.3 = f32[256,256]{1,0:T(8,128)S(1)} copy-done((f32[256,256]{1,0:T(8,128)S(1)}, f32[256,256]{1,0:T(8,128)}, u32[]{:S(2)}) %copy-start.3) | copy-done | bytes 262168
  5.7 3.1 %collective-permute-start.22 = (f32[512,256]{1,0:T(8,128)S(1)}, f32[512,256]{1,0:T(8,128)S(1)}, u32[]{:S(2)}, u32[]{:S(2)}) collective-permute-start(f32[512,256]{1,0:T(8,128)S(1)} %pack_rows.1.refs_8_), channel_id=1, source_target_pairs={{0,16},{8,24},{16,0},{24,8},{1,17},{9,25},{17,1},{25,9},{2,18},{10... | collective-permute-start | bytes 1572872 | tf_op jit(solution)/shard_map/ppermute | solution.py:20
  8.8 1.5 %collective-permute-start.21 = (f32[512,256]{1,0:T(8,128)S(1)}, f32[512,256]{1,0:T(8,128)}, u32[]{:S(2)}, u32[]{:S(2)}) collective-permute-start(f32[512,256]{1,0:T(8,128)S(1)} %pack_rows.1.refs_8_), channel_id=1, source_target_pairs={{0,8},{8,0},{16,24},{24,16},{1,9},{9,1},{17,25},{25,17},{2,10},{10... | collective-permute-start | bytes 1572872 | tf_op jit(solution)/shard_map/ppermute | solution.py:20
  10.3 1.6 %fusion.41 = f32[2048,128]{1,0:T(8,128)S(1)} fusion(bf16[2048,512]{1,0:T(8,128)(2,1)S(1)} %copy-done, bf16[512,128]{1,0:T(8,128)(2,1)} %refs_6_.1), kind=kOutput, calls=%fused_computation.69 | convolution fusion | flops 268435456 | bytes 3276800 | tf_op jit(solution)/shard_map/dot_general | solution.py:341
  12.9 1.9 %collective-permute-start.1 = (f16[144,256]{1,0:T(8,128)(2,1)S(1)}, f16[144,256]{1,0:T(8,128)(2,1)}, u32[]{:S(2)}, u32[]{:S(2)}) collective-permute-start(f16[144,256]{1,0:T(8,128)(2,1)S(1)} %convert_element_type.110), channel_id=1, source_target_pairs={{0,16},{8,24},{16,0},{24,8},{1,17},{9,25},{17,1},{25,9},{2,18},{10... | collective-permute-start | bytes 221192 | tf_op jit(solution)/shard_map/ppermute | solution.py:20
  15.0 1.6 %partial_first.1 = (f32[1024,128]{1,0:T(8,128)S(1)}, f32[16,128]{1,0:T(8,128)S(1)}) custom-call(bf16[2048,128]{1,0:T(8,128)(2,1)} %heads.1, bf16[256,128]{1,0:T(8,128)(2,1)S(1)} %constant_dynamic-slice_fusion.factor), custom_call_target="tpu_custom_call" | custom-call | flops 200000000 | tf_op jit(solution)/shard_map/partial_first/pallas_call | solution.py:215
  16.5 7.2 %collective-permute-done.2 = f16[144,256]{1,0:T(8,128)(2,1)} collective-permute-done((f16[144,256]{1,0:T(8,128)(2,1)S(1)}, f16[144,256]{1,0:T(8,128)(2,1)}, u32[]{:S(2)}, u32[]{:S(2)}) %collective-permute-start.2) | collective-permute-done | bytes 73760 | tf_op jit(solution)/shard_map/ppermute | solution.py:20
  23.8 1.6 %collective-permute-start = (f16[144,256]{1,0:T(8,128)(2,1)S(1)}, f16[144,256]{1,0:T(8,128)(2,1)S(1)}, u32[]{:S(2)}, u32[]{:S(2)}) collective-permute-start(f16[144,256]{1,0:T(8,128)(2,1)S(1)} %convert_element_type.110), channel_id=1, source_target_pairs={{0,8},{8,0},{16,24},{24,16},{1,9},{9,1},{17,25},{25,17},{2,10},{10... | collective-permute-start | bytes 221192 | tf_op jit(solution)/shard_map/ppermute | solution.py:20
  26.8 1.3 %collective-permute-done = f16[144,256]{1,0:T(8,128)(2,1)S(1)} collective-permute-done((f16[144,256]{1,0:T(8,128)(2,1)S(1)}, f16[144,256]{1,0:T(8,128)(2,1)S(1)}, u32[]{:S(2)}, u32[]{:S(2)}) %collective-permute-start) | collective-permute-done | bytes 73760 | tf_op jit(solution)/shard_map/ppermute | solution.py:20
  28.1 1.5 %partial_second.1 = (f32[256,128]{1,0:T(8,128)S(1)}, f32[272,128]{1,0:T(8,128)S(1)}, f32[272,128]{1,0:T(8,128)S(1)}, f32[272,128]{1,0:T(8,128)S(1)}, f32[16,128]{1,0:T(8,128)S(1)}) custom-call(bf16[2048,128]{1,0:T(8,128)(2,1)} %collective-permute-done.3.heads, f32[1024,128]{1,0:T(8,128)S(1)} %get-tuple-element.17.parts, ...), custom_call_target="tpu_custom_call" | custom-call | flops 200000000 | tf_op jit(solution)/shard_map/partial_second/pallas_call | solution.py:227
  29.7 3.8 %collective-permute-start.6 = (f16[272,128]{1,0:T(8,128)(2,1)S(1)}, f16[272,128]{1,0:T(8,128)(2,1)S(1)}, u32[]{:S(2)}, u32[]{:S(2)}) collective-permute-start(f16[272,128]{1,0:T(8,128)(2,1)S(1)} %convert_element_type.127), channel_id=1, source_target_pairs={{0,6},{1,7},{2,4},{3,5},{4,2},{5,3},{6,0},{7,1},{8,14},{9,15},{10,... | collective-permute-start | bytes 208904 | tf_op jit(solution)/shard_map/ppermute | solution.py:20
  35.1 1.7 %collective-permute-start.24 = (f32[256,256]{1,0:T(8,128)S(1)}, f32[256,256]{1,0:T(8,128)S(1)}, u32[]{:S(2)}, u32[]{:S(2)}) collective-permute-start(f32[256,256]{1,0:T(8,128)S(1)} %slice.146), channel_id=1, source_target_pairs={{0,8},{8,0},{16,24},{24,16},{1,9},{9,1},{17,25},{25,17},{2,10},{10... | collective-permute-start | bytes 786440 | tf_op jit(solution)/shard_map/ppermute | solution.py:20
  36.8 1.0 %slice.145 = f32[256,256]{1,0:T(8,128)S(1)} slice(f32[512,256]{1,0:T(8,128)} %collective-permute-done.21.refs_9_), slice={[0:256], [0:256]} | slice | bytes 524288 | tf_op jit(solution)/shard_map/slice | solution.py:334
  37.8 1.6 %collective-permute-start.23 = (f32[256,256]{1,0:T(8,128)S(1)}, f32[256,256]{1,0:T(8,128)S(1)}, u32[]{:S(2)}, u32[]{:S(2)}) collective-permute-start(f32[256,256]{1,0:T(8,128)S(1)} %slice.145), channel_id=1, source_target_pairs={{0,16},{8,24},{16,0},{24,8},{1,17},{9,25},{17,1},{25,9},{2,18},{10... | collective-permute-start | bytes 786440 | tf_op jit(solution)/shard_map/ppermute | solution.py:20
  39.5 3.7 %collective-permute-start.12 = (f16[256,128]{1,0:T(8,128)(2,1)S(1)}, f16[256,128]{1,0:T(8,128)(2,1)S(1)}, u32[]{:S(2)}, u32[]{:S(2)}) collective-permute-start(f16[256,128]{1,0:T(8,128)(2,1)S(1)} %multiply_convert_fusion), channel_id=1, source_target_pairs={{0,6},{1,7},{2,4},{3,5},{4,2},{5,3},{6,0},{7,1},{8,14},{9,15},{10,... | collective-permute-start | bytes 196616 | tf_op jit(solution)/shard_map/ppermute | solution.py:20
  44.2 4.1 %collective-permute-done.10 = f16[256,128]{1,0:T(8,128)(2,1)S(1)} collective-permute-done((f16[256,128]{1,0:T(8,128)(2,1)S(1)}, f16[256,128]{1,0:T(8,128)(2,1)S(1)}, u32[]{:S(2)}, u32[]{:S(2)}) %collective-permute-start.10) | collective-permute-done | bytes 65568 | tf_op jit(solution)/shard_map/ppermute | solution.py:20
  51.8 1.8 %collective-permute-start.16 = (f16[144,256]{1,0:T(8,128)(2,1)S(1)}, f16[144,256]{1,0:T(8,128)(2,1)S(1)}, u32[]{:S(2)}, u32[]{:S(2)}) collective-permute-start(f16[144,256]{1,0:T(8,128)(2,1)S(1)} %convert_element_type.132), channel_id=1, source_target_pairs={{0,24},{8,16},{16,8},{24,0},{1,25},{9,17},{17,9},{25,1},{2,26},{10... | collective-permute-start | bytes 221192 | tf_op jit(solution)/shard_map/ppermute | solution.py:20
  54.1 1.3 %collective-permute-start.14 = (f16[144,256]{1,0:T(8,128)(2,1)S(1)}, f16[144,256]{1,0:T(8,128)(2,1)S(1)}, u32[]{:S(2)}, u32[]{:S(2)}) collective-permute-start(f16[144,256]{1,0:T(8,128)(2,1)S(1)} %convert_element_type.132), channel_id=1, source_target_pairs={{0,8},{8,0},{16,24},{24,16},{1,9},{9,1},{17,25},{25,17},{2,10},{10... | collective-permute-start | bytes 221192 | tf_op jit(solution)/shard_map/ppermute | solution.py:20
  55.4 1.8 %collective-permute-done.16 = f16[144,256]{1,0:T(8,128)(2,1)S(1)} collective-permute-done((f16[144,256]{1,0:T(8,128)(2,1)S(1)}, f16[144,256]{1,0:T(8,128)(2,1)S(1)}, u32[]{:S(2)}, u32[]{:S(2)}) %collective-permute-start.16) | collective-permute-done | bytes 73760 | tf_op jit(solution)/shard_map/ppermute | solution.py:20
  57.2 1.5 %collective-permute-done.15 = f16[144,256]{1,0:T(8,128)(2,1)S(1)} collective-permute-done((f16[144,256]{1,0:T(8,128)(2,1)S(1)}, f16[144,256]{1,0:T(8,128)(2,1)S(1)}, u32[]{:S(2)}, u32[]{:S(2)}) %collective-permute-start.15) | collective-permute-done | bytes 73760 | tf_op jit(solution)/shard_map/ppermute | solution.py:20
  58.9 1.1 %collective-permute-done.17.b = f32[8,128]{1,0:T(8,128)S(1)} collective-permute-done((f32[8,128]{1,0:T(8,128)S(1)}, f32[8,128]{1,0:T(8,128)S(1)}, u32[]{:S(2)}, u32[]{:S(2)}) %collective-permute-start.17) | collective-permute-done | bytes 4128 | tf_op jit(solution)/shard_map/ppermute | solution.py:20
  60.0 2.4 %collective-permute-start.19 = (f32[8,128]{1,0:T(8,128)S(1)}, f32[8,128]{1,0:T(8,128)S(1)}, u32[]{:S(2)}, u32[]{:S(2)}) collective-permute-start(f32[8,128]{1,0:T(8,128)S(1)} %add_tiles.1.refs_0_), channel_id=1, source_target_pairs={{0,4},{1,5},{2,6},{3,7},{4,0},{5,1},{6,2},{7,3},{8,12},{9,13},{10,... | collective-permute-start | bytes 12296 | tf_op jit(solution)/shard_map/ppermute | solution.py:20
  62.4 1.2 %collective-permute-done.18.refs_1_ = f32[8,128]{1,0:T(8,128)S(1)} collective-permute-done((f32[8,128]{1,0:T(8,128)S(1)}, f32[8,128]{1,0:T(8,128)S(1)}, u32[]{:S(2)}, u32[]{:S(2)}) %collective-permute-start.18) | collective-permute-done | bytes 4128 | tf_op jit(solution)/shard_map/ppermute | solution.py:24
  65.3 2.8 %finish.1 = (f32[128,256]{1,0:T(8,128)}, f32[128,256]{1,0:T(8,128)}, bf16[512,256]{1,0:T(8,128)(2,1)}, f32[32,256]{1,0:T(8,128)}, f32[32,256]{1,0:T(8,128)}, /*i...) custom-call(f32[8,128]{1,0:T(8,128)S(1)} %add_tiles.1.refs_0_, ...), custom_call_target="tpu_custom_call" | custom-call | tf_op jit(solution)/shard_map/finish/pallas_call | solution.py:105
  (86 shorter events, 14.8 us)
Async XLA Ops:
  5.7 29.4 %collective-permute-start.22 = (f32[512,256]{1,0:T(8,128)S(1)}, f32[512,256]{1,0:T(8,128)S(1)}, u32[]{:S(2)}, u32[]{:S(2)}) collective-permute-start(f32[512,256]{1,0:T(8,128)S(1)} %pack_rows.1.refs_8_), channel_id=1, source_target_pairs={{0,16},{8,24},{16,0},{24,8},{1,17},{9,25},{17,1},{25,9},{2,18},{10... | collective-permute-start | bytes 1572872 | tf_op jit(solution)/shard_map/ppermute | solution.py:20
  8.8 28.0 %collective-permute-start.21 = (f32[512,256]{1,0:T(8,128)S(1)}, f32[512,256]{1,0:T(8,128)}, u32[]{:S(2)}, u32[]{:S(2)}) collective-permute-start(f32[512,256]{1,0:T(8,128)S(1)} %pack_rows.1.refs_8_), channel_id=1, source_target_pairs={{0,8},{8,0},{16,24},{24,16},{1,9},{9,1},{17,25},{25,17},{2,10},{10... | collective-permute-start | bytes 1572872 | tf_op jit(solution)/shard_map/ppermute | solution.py:20
  12.8 11.0 %collective-permute-start.2 = (f16[144,256]{1,0:T(8,128)(2,1)S(1)}, f16[144,256]{1,0:T(8,128)(2,1)}, u32[]{:S(2)}, u32[]{:S(2)}) collective-permute-start(f16[144,256]{1,0:T(8,128)(2,1)S(1)} %convert_element_type.110), channel_id=1, source_target_pairs={{0,24},{8,16},{16,8},{24,0},{1,25},{9,17},{17,9},{25,1},{2,26},{10... | collective-permute-start | bytes 221192 | tf_op jit(solution)/shard_map/ppermute | solution.py:20
  12.9 13.2 %collective-permute-start.1 = (f16[144,256]{1,0:T(8,128)(2,1)S(1)}, f16[144,256]{1,0:T(8,128)(2,1)}, u32[]{:S(2)}, u32[]{:S(2)}) collective-permute-start(f16[144,256]{1,0:T(8,128)(2,1)S(1)} %convert_element_type.110), channel_id=1, source_target_pairs={{0,16},{8,24},{16,0},{24,8},{1,17},{9,25},{17,1},{25,9},{2,18},{10... | collective-permute-start | bytes 221192 | tf_op jit(solution)/shard_map/ppermute | solution.py:20
  14.9 13.3 %collective-permute-start.3 = (bf16[2048,128]{1,0:T(8,128)(2,1)}, bf16[2048,128]{1,0:T(8,128)(2,1)}, u32[]{:S(2)}, u32[]{:S(2)}) collective-permute-start(bf16[2048,128]{1,0:T(8,128)(2,1)} %heads.1), channel_id=1, source_target_pairs={{0,1},{1,0},{2,3},{3,2},{4,5},{5,4},{6,7},{7,6},{8,9},{9,8},{10,11... | collective-permute-start | bytes 1572872 | tf_op jit(solution)/shard_map/ppermute | solution.py:20
  23.8 4.4 %collective-permute-start = (f16[144,256]{1,0:T(8,128)(2,1)S(1)}, f16[144,256]{1,0:T(8,128)(2,1)S(1)}, u32[]{:S(2)}, u32[]{:S(2)}) collective-permute-start(f16[144,256]{1,0:T(8,128)(2,1)S(1)} %convert_element_type.110), channel_id=1, source_target_pairs={{0,8},{8,0},{16,24},{24,16},{1,9},{9,1},{17,25},{25,17},{2,10},{10... | collective-permute-start | bytes 221192 | tf_op jit(solution)/shard_map/ppermute | solution.py:20
  29.7 9.7 %collective-permute-start.6 = (f16[272,128]{1,0:T(8,128)(2,1)S(1)}, f16[272,128]{1,0:T(8,128)(2,1)S(1)}, u32[]{:S(2)}, u32[]{:S(2)}) collective-permute-start(f16[272,128]{1,0:T(8,128)(2,1)S(1)} %convert_element_type.127), channel_id=1, source_target_pairs={{0,6},{1,7},{2,4},{3,5},{4,2},{5,3},{6,0},{7,1},{8,14},{9,15},{10,... | collective-permute-start | bytes 208904 | tf_op jit(solution)/shard_map/ppermute | solution.py:20
  33.5 5.9 %collective-permute-start.5 = (f16[272,128]{1,0:T(8,128)(2,1)S(1)}, f16[272,128]{1,0:T(8,128)(2,1)S(1)}, u32[]{:S(2)}, u32[]{:S(2)}) collective-permute-start(f16[272,128]{1,0:T(8,128)(2,1)S(1)} %convert_element_type.123), channel_id=1, source_target_pairs={{0,4},{1,5},{2,6},{3,7},{4,0},{5,1},{6,2},{7,3},{8,12},{9,13},{10,... | collective-permute-start | bytes 208904 | tf_op jit(solution)/shard_map/ppermute | solution.py:20
  33.5 5.9 %collective-permute-start.4 = (f16[272,128]{1,0:T(8,128)(2,1)S(1)}, f16[272,128]{1,0:T(8,128)(2,1)S(1)}, u32[]{:S(2)}, u32[]{:S(2)}) collective-permute-start(f16[272,128]{1,0:T(8,128)(2,1)S(1)} %convert_element_type.119), channel_id=1, source_target_pairs={{0,2},{1,3},{2,0},{3,1},{4,6},{5,7},{6,4},{7,5},{8,10},{9,11},{10,... | collective-permute-start | bytes 208904 | tf_op jit(solution)/shard_map/ppermute | solution.py:20
  35.1 29.3 %collective-permute-start.24 = (f32[256,256]{1,0:T(8,128)S(1)}, f32[256,256]{1,0:T(8,128)S(1)}, u32[]{:S(2)}, u32[]{:S(2)}) collective-permute-start(f32[256,256]{1,0:T(8,128)S(1)} %slice.146), channel_id=1, source_target_pairs={{0,8},{8,0},{16,24},{24,16},{1,9},{9,1},{17,25},{25,17},{2,10},{10... | collective-permute-start | bytes 786440 | tf_op jit(solution)/shard_map/ppermute | solution.py:20
  37.8 26.7 %collective-permute-start.23 = (f32[256,256]{1,0:T(8,128)S(1)}, f32[256,256]{1,0:T(8,128)S(1)}, u32[]{:S(2)}, u32[]{:S(2)}) collective-permute-start(f32[256,256]{1,0:T(8,128)S(1)} %slice.145), channel_id=1, source_target_pairs={{0,16},{8,24},{16,0},{24,8},{1,17},{9,25},{17,1},{25,9},{2,18},{10... | collective-permute-start | bytes 786440 | tf_op jit(solution)/shard_map/ppermute | solution.py:20
  39.5 9.1 %collective-permute-start.12 = (f16[256,128]{1,0:T(8,128)(2,1)S(1)}, f16[256,128]{1,0:T(8,128)(2,1)S(1)}, u32[]{:S(2)}, u32[]{:S(2)}) collective-permute-start(f16[256,128]{1,0:T(8,128)(2,1)S(1)} %multiply_convert_fusion), channel_id=1, source_target_pairs={{0,6},{1,7},{2,4},{3,5},{4,2},{5,3},{6,0},{7,1},{8,14},{9,15},{10,... | collective-permute-start | bytes 196616 | tf_op jit(solution)/shard_map/ppermute | solution.py:20
  43.2 5.2 %collective-permute-start.10 = (f16[256,128]{1,0:T(8,128)(2,1)S(1)}, f16[256,128]{1,0:T(8,128)(2,1)S(1)}, u32[]{:S(2)}, u32[]{:S(2)}) collective-permute-start(f16[256,128]{1,0:T(8,128)(2,1)S(1)} %multiply_convert_fusion), channel_id=1, source_target_pairs={{0,4},{1,5},{2,6},{3,7},{4,0},{5,1},{6,2},{7,3},{8,12},{9,13},{10,... | collective-permute-start | bytes 196616 | tf_op jit(solution)/shard_map/ppermute | solution.py:20
  43.2 6.0 %collective-permute-start.8 = (f16[256,128]{1,0:T(8,128)(2,1)S(1)}, f16[256,128]{1,0:T(8,128)(2,1)S(1)}, u32[]{:S(2)}, u32[]{:S(2)}) collective-permute-start(f16[256,128]{1,0:T(8,128)(2,1)S(1)} %multiply_convert_fusion), channel_id=1, source_target_pairs={{0,2},{1,3},{2,0},{3,1},{4,6},{5,7},{6,4},{7,5},{8,10},{9,11},{10,... | collective-permute-start | bytes 196616 | tf_op jit(solution)/shard_map/ppermute | solution.py:20
  48.3 1.3 %collective-permute-start.7 = (f16[256,128]{1,0:T(8,128)(2,1)S(1)}, f16[256,128]{1,0:T(8,128)(2,1)S(1)}, u32[]{:S(2)}, u32[]{:S(2)}) collective-permute-start(f16[256,128]{1,0:T(8,128)(2,1)S(1)} %multiply_convert_fusion), channel_id=1, source_target_pairs={{0,1},{1,0},{2,3},{3,2},{4,5},{5,4},{6,7},{7,6},{8,9},{9,8},{10,11... | collective-permute-start | bytes 196616 | tf_op jit(solution)/shard_map/ppermute | solution.py:20
  48.6 2.5 %collective-permute-start.11 = (f16[256,128]{1,0:T(8,128)(2,1)S(1)}, f16[256,128]{1,0:T(8,128)(2,1)S(1)}, u32[]{:S(2)}, u32[]{:S(2)}) collective-permute-start(f16[256,128]{1,0:T(8,128)(2,1)S(1)} %collective-permute-done.10), channel_id=1, source_target_pairs={{0,1},{1,0},{2,3},{3,2},{4,5},{5,4},{6,7},{7,6},{8,9},{9,8},{10,11... | collective-permute-start | bytes 196616 | tf_op jit(solution)/shard_map/ppermute | solution.py:20
  49.2 2.2 %collective-permute-start.13 = (f16[256,128]{1,0:T(8,128)(2,1)S(1)}, f16[256,128]{1,0:T(8,128)(2,1)S(1)}, u32[]{:S(2)}, u32[]{:S(2)}) collective-permute-start(f16[256,128]{1,0:T(8,128)(2,1)S(1)} %collective-permute-done.12), channel_id=1, source_target_pairs={{0,1},{1,0},{2,3},{3,2},{4,5},{5,4},{6,7},{7,6},{8,9},{9,8},{10,11... | collective-permute-start | bytes 196616 | tf_op jit(solution)/shard_map/ppermute | solution.py:20
  49.6 1.3 %collective-permute-start.9 = (f16[256,128]{1,0:T(8,128)(2,1)S(1)}, f16[256,128]{1,0:T(8,128)(2,1)S(1)}, u32[]{:S(2)}, u32[]{:S(2)}) collective-permute-start(f16[256,128]{1,0:T(8,128)(2,1)S(1)} %collective-permute-done.8), channel_id=1, source_target_pairs={{0,1},{1,0},{2,3},{3,2},{4,5},{5,4},{6,7},{7,6},{8,9},{9,8},{10,11... | collective-permute-start | bytes 196616 | tf_op jit(solution)/shard_map/ppermute | solution.py:20
  51.8 5.4 %collective-permute-start.16 = (f16[144,256]{1,0:T(8,128)(2,1)S(1)}, f16[144,256]{1,0:T(8,128)(2,1)S(1)}, u32[]{:S(2)}, u32[]{:S(2)}) collective-permute-start(f16[144,256]{1,0:T(8,128)(2,1)S(1)} %convert_element_type.132), channel_id=1, source_target_pairs={{0,24},{8,16},{16,8},{24,0},{1,25},{9,17},{17,9},{25,1},{2,26},{10... | collective-permute-start | bytes 221192 | tf_op jit(solution)/shard_map/ppermute | solution.py:20
  53.6 5.1 %collective-permute-start.15 = (f16[144,256]{1,0:T(8,128)(2,1)S(1)}, f16[144,256]{1,0:T(8,128)(2,1)S(1)}, u32[]{:S(2)}, u32[]{:S(2)}) collective-permute-start(f16[144,256]{1,0:T(8,128)(2,1)S(1)} %convert_element_type.132), channel_id=1, source_target_pairs={{0,16},{8,24},{16,0},{24,8},{1,17},{9,25},{17,1},{25,9},{2,18},{10... | collective-permute-start | bytes 221192 | tf_op jit(solution)/shard_map/ppermute | solution.py:20
  54.1 4.6 %collective-permute-start.14 = (f16[144,256]{1,0:T(8,128)(2,1)S(1)}, f16[144,256]{1,0:T(8,128)(2,1)S(1)}, u32[]{:S(2)}, u32[]{:S(2)}) collective-permute-start(f16[144,256]{1,0:T(8,128)(2,1)S(1)} %convert_element_type.132), channel_id=1, source_target_pairs={{0,8},{8,0},{16,24},{24,16},{1,9},{9,1},{17,25},{25,17},{2,10},{10... | collective-permute-start | bytes 221192 | tf_op jit(solution)/shard_map/ppermute | solution.py:20
  60.0 3.6 %collective-permute-start.18 = (f32[8,128]{1,0:T(8,128)S(1)}, f32[8,128]{1,0:T(8,128)S(1)}, u32[]{:S(2)}, u32[]{:S(2)}) collective-permute-start(f32[8,128]{1,0:T(8,128)S(1)} %add_tiles.1.refs_0_), channel_id=1, source_target_pairs={{0,2},{1,7},{2,0},{3,5},{4,6},{5,3},{6,4},{7,1},{8,10},{9,15},{10,... | collective-permute-start | bytes 12296 | tf_op jit(solution)/shard_map/ppermute | solution.py:24
  60.0 4.5 %collective-permute-start.19 = (f32[8,128]{1,0:T(8,128)S(1)}, f32[8,128]{1,0:T(8,128)S(1)}, u32[]{:S(2)}, u32[]{:S(2)}) collective-permute-start(f32[8,128]{1,0:T(8,128)S(1)} %add_tiles.1.refs_0_), channel_id=1, source_target_pairs={{0,4},{1,5},{2,6},{3,7},{4,0},{5,1},{6,2},{7,3},{8,12},{9,13},{10,... | collective-permute-start | bytes 12296 | tf_op jit(solution)/shard_map/ppermute | solution.py:20
  63.6 1.6 %collective-permute-start.20 = (f32[8,128]{1,0:T(8,128)S(1)}, f32[8,128]{1,0:T(8,128)S(1)}, u32[]{:S(2)}, u32[]{:S(2)}) collective-permute-start(f32[8,128]{1,0:T(8,128)S(1)} %collective-permute-done.18.refs_1_), channel_id=1, source_target_pairs={{0,1},{1,0},{2,3},{3,2},{4,5},{5,4},{6,7},{7,6},{8,9},{9,8},{10,11... | collective-permute-start | bytes 12296 | tf_op jit(solution)/shard_map/ppermute | solution.py:20
  (12 other events, 70.7 us)

commit v2 on v1

--- a/solution.py
+++ b/solution.py
@@ -161,6 +161,14 @@
     return jnp.max(jnp.max(jnp.abs(x[...]).astype(f32), axis=0, keepdims=True), axis=1, keepdims=True)
 
 
+def chunks_of(core, chip, chips, half, chunk):
+    offsets = [core * half + (chip ^ k) * chunk for k in range(chips)]
+    if chips == 4:
+        split = (chip ^ (1 + 2 * core)) * chunk
+        offsets = [offsets[0], core * half + split, (1 - core) * half + split, offsets[2]]
+    return [pl.multiple_of(at, chunk) for at in offsets]
+
+
 def first_kernel(chips, heads, factor, parts, rows_out):
     tokens, features = heads.shape
     half, rank = tokens // 2, factor.shape[1]
@@ -168,8 +176,7 @@
     place = lax.axis_index("tp")
     core, chip = place & 1, place >> 1
     own_factor = factor[pl.ds(pl.multiple_of(core * features, features), features), :]
-    for k in range(chips):
-        at = pl.multiple_of(core * half + (chip ^ k) * chunk, chunk)
+    for k, at in enumerate(chunks_of(core, chip, chips, half, chunk)):
         parts[k * chunk : (k + 1) * chunk, :] = jnp.dot(
             heads[pl.ds(at, chunk), :], own_factor, preferred_element_type=f32
         )
@@ -189,17 +196,20 @@
     )
     scale = 1.0 / (largest * rows[8:9, :] * term_bound(features))
     other_factor = factor[pl.ds(pl.multiple_of((core ^ 1) * features, features), features), :]
-    for k in reversed(range(chips)):
-        at = pl.multiple_of(core * half + (chip ^ k) * chunk, chunk)
+    own, *sends, marks_out = outs
+    places = [(0, 0), (0, chunk), (1, 0)] if chips == 4 else [(k, 0) for k in range(chips - 1)]
+    for k, at in enumerate(chunks_of(core, chip, chips, half, chunk)):
         part = parts[k * chunk : (k + 1) * chunk, :] + jnp.dot(
             heads[pl.ds(at, chunk), :], other_factor, preferred_element_type=f32
         )
         if k == 0:
-            outs[0][...] = part
+            own[...] = part
         else:
-            outs[k][0:chunk, :] = part * scale
-            outs[k][chunk : chunk + 16, :] = marks
-    outs[chips][...] = marks
+            which, row = places[k - 1]
+            sends[which][row : row + chunk, :] = part * scale
+    for send in sends:
+        send[send.shape[0] - 16 : send.shape[0], :] = marks
+    marks_out[...] = marks
 
 
 def term_bound(features):
@@ -210,6 +220,7 @@
     tokens, _ = heads.shape
     rank = factor.shape[1]
     chunk = tokens // (2 * chips)
+    lengths = [2 * chunk + 16, chunk + 16] if chips == 4 else [chunk + 16] * (chips - 1)
     vmem = pl.BlockSpec(memory_space=pltpu.VMEM)
     cost = pl.CostEstimate(flops=200_000_000, bytes_accessed=0, transcendentals=0)
     parts, rows = pl.pallas_call(
@@ -226,11 +237,9 @@
     )(heads, factor)
     return pl.pallas_call(
         functools.partial(second_kernel, chips),
-        out_shape=[jax.ShapeDtypeStruct((chunk, rank), f32)]
-        + [jax.ShapeDtypeStruct((chunk + 16, rank), f32)] * (chips - 1)
-        + [jax.ShapeDtypeStruct((16, rank), f32)],
+        out_shape=[jax.ShapeDtypeStruct((n, rank), f32) for n in (chunk, *lengths, 16)],
         in_specs=[vmem] * 4,
-        out_specs=[vmem] * (chips + 1),
+        out_specs=[vmem] * (2 + len(lengths)),
         compiler_params=SMALL,
         cost_estimate=cost,
         name="partial_second",
@@ -349,8 +358,15 @@
     )
     strength = scale_rows[0:1] * scale_rows[8:9]
     arrived = []
-    for k in range(1, chips):
-        arrived.append(send_xor(sends[k - 1].astype(f16), "tp", 2 * k))
+    sends = [send.astype(f16) for send in sends]
+    if chips == 4:
+        halves = send_split(sends[0])
+        arrived.append(send_xor(sends[1], "tp", 4))
+        arrived.append(send_xor(halves[chunk:], "tp", 1))
+        arrived.append(jnp.concatenate([halves[:chunk], halves[2 * chunk :]], axis=0))
+    else:
+        for k in range(1, chips):
+            arrived.append(send_xor(sends[k - 1], "tp", 2 * k))
     for a in arrived:
         of_peer = a[chunk : chunk + 1].astype(f32) * a[chunk + 8 : chunk + 9].astype(f32)
         strength = jnp.maximum(strength, of_peer)
@@ -358,14 +374,19 @@
     bound_total = chips * term_bound(features) * strength
     total = (total * (1.0 / bound_total)).astype(f16)
 
-    products = []
-    for k in range(chips):
-        mine = send_xor(total, "tp", 2 * k) if k else total
+    def product(part, at):
+        rows = lax.dynamic_slice_in_dim(output_cotangent, at, chunk, 0)
+        return project(part.astype(f32), rows)
+
+    here, there = core * half, (1 - core) * half
+    theirs = send_xor(total, "tp", 1)
+    products = [product(total, here + chip * chunk)]
+    products.append(product(theirs, there + chip * chunk))
+    for k in range(1, chips):
+        mine = send_xor(total, "tp", 2 * k)
         theirs = send_xor(mine, "tp", 1)
-        for at, part in ((core * half, mine), ((1 - core) * half, theirs)):
-            rows = lax.dynamic_slice_in_dim(output_cotangent, at + (chip ^ k) * chunk, chunk, 0)
-            product = project(part.astype(f32), rows)
-            products.append(product)
+        products.append(product(mine, here + (chip ^ k) * chunk))
+        products.append(product(theirs, there + (chip ^ k) * chunk))
     output_term = sum(products[1:], products[0]) * bound_total[0, 0]
 
     value_proj = sum_fs(value_term)

time: 68.8 us -> 69.5 us (1.010)
  waiting for transfers between devices: 19.9 us -> 21.2 us
  starting transfers between devices: 28.1 us -> 27.4 us
    ppermute x24 -> x23, starting transfers between devices: 28.1 us -> 25.7 us  [send_xor(): return lax.ppermute(x, axis, [(i, i ^ step) for i in range(count)])]
    ppermute x1 -> x2, waiting for transfers between devices: 1.21 us -> 3.38 us  [send_split(): lax.ppermute(x, 'tp', [(i, i ^ (6 if i & 1 else 2)) for i in range(8)])]
    ppermute x1 -> x2, starting transfers between devices: 0.01 us -> 1.65 us  [send_split(): lax.ppermute(x, 'tp', [(i, i ^ (6 if i & 1 else 2)) for i in range(8)])]
    ppermute x24 -> x23, waiting for transfers between devices: 18.7 us -> 17.9 us  [send_xor(): return lax.ppermute(x, axis, [(i, i ^ step) for i in range(count)])]
  transfers between devices with their start and end apart: 25 -> 25, of which waited for: 11 -> 12; matrix products, arithmetic and copies ran while one was open for 12% -> 11% of each run, Pallas kernels for 5% -> 5%
where the time goes in v2:
time: 69.5 us; the launch traced here: 68.8 us
  starting transfers between devices  27.4 us (39%)
  waiting for transfers between devices  21.2 us (31%)
  Pallas kernels  6.26 us (9%)
  local copies, waits for them, and re-layouts  6.07 us (9%)
  matrix products  4.36 us (6%)
  other arithmetic  2.5 us (4%)
  between operations  1 us (1%)
    ppermute x23, starting transfers between devices, send_xor(): return lax.ppermute(x, axis, [(i, i ^ step) for i in range(count)])  25.7 us
    ppermute x23, waiting for transfers between devices, send_xor(): return lax.ppermute(x, axis, [(i, i ^ step) for i in range(count)])  17.9 us
    unnamed x22, local copies, waits for them, and re-layouts  5.06 us
    ppermute x2, waiting for transfers between devices, send_split(): lax.ppermute(x, 'tp', [(i, i ^ (6 if i & 1 else 2)) for i in range(8)])  3.38 us
    pallas_call x1, Pallas kernels, finish(): pl.pallas_call(functools.partial(finish_kernel, len(tiles), places, entri...  2.81 us
    dot_general x9, matrix products, project(): lax.dot_general(image, cotangent.astype(f32), (((0,), (0,)), ((), ())), p...  2.76 us
    ppermute x2, starting transfers between devices, send_split(): lax.ppermute(x, 'tp', [(i, i ^ (6 if i & 1 else 2)) for i in range(8)])  1.65 us
    dot_general x1, matrix products, on_device(): jnp.dot(value_cotangent, value_factor, preferred_element_type=f32)  1.6 us
  transfers between devices with their start and end apart: 25, of which 12 were waited for; matrix products, arithmetic and copies ran while one was open for 11% of the time, Pallas kernels for 5%

profile of v2, /device:TPU:0, one launch (start us, length us, event | category | flops | bytes accessed | tf_op | source)
XLA Modules:
  0.0 68.8 jit_solution(5611608816888325267)
XLA Ops:
  0.7 1.1 %copy-done.3 = f32[256,256]{1,0:T(8,128)S(1)} copy-done((f32[256,256]{1,0:T(8,128)S(1)}, f32[256,256]{1,0:T(8,128)}, u32[]{:S(2)}) %copy-start.3) | copy-done | bytes 262168
  5.7 3.1 %collective-permute-start.22 = (f32[512,256]{1,0:T(8,128)S(1)}, f32[512,256]{1,0:T(8,128)S(1)}, u32[]{:S(2)}, u32[]{:S(2)}) collective-permute-start(f32[512,256]{1,0:T(8,128)S(1)} %pack_rows.1.refs_8_), channel_id=1, source_target_pairs={{0,16},{8,24},{16,0},{24,8},{1,17},{9,25},{17,1},{25,9},{2,18},{10... | collective-permute-start | bytes 1572872 | tf_op jit(solution)/shard_map/ppermute | solution.py:20
  8.8 1.5 %collective-permute-start.21 = (f32[512,256]{1,0:T(8,128)S(1)}, f32[512,256]{1,0:T(8,128)}, u32[]{:S(2)}, u32[]{:S(2)}) collective-permute-start(f32[512,256]{1,0:T(8,128)S(1)} %pack_rows.1.refs_8_), channel_id=1, source_target_pairs={{0,8},{8,0},{16,24},{24,16},{1,9},{9,1},{17,25},{25,17},{2,10},{10... | collective-permute-start | bytes 1572872 | tf_op jit(solution)/shard_map/ppermute | solution.py:20
  10.3 1.6 %fusion.41 = f32[2048,128]{1,0:T(8,128)S(1)} fusion(bf16[2048,512]{1,0:T(8,128)(2,1)S(1)} %copy-done, bf16[512,128]{1,0:T(8,128)(2,1)} %refs_6_.1), kind=kOutput, calls=%fused_computation.69 | convolution fusion | flops 268435456 | bytes 3276800 | tf_op jit(solution)/shard_map/dot_general | solution.py:350
  12.9 1.9 %collective-permute-start.1 = (f16[144,256]{1,0:T(8,128)(2,1)S(1)}, f16[144,256]{1,0:T(8,128)(2,1)}, u32[]{:S(2)}, u32[]{:S(2)}) collective-permute-start(f16[144,256]{1,0:T(8,128)(2,1)S(1)} %convert_element_type.107), channel_id=1, source_target_pairs={{0,16},{8,24},{16,0},{24,8},{1,17},{9,25},{17,1},{25,9},{2,18},{10... | collective-permute-start | bytes 221192 | tf_op jit(solution)/shard_map/ppermute | solution.py:20
  15.0 1.6 %partial_first.1 = (f32[1024,128]{1,0:T(8,128)S(1)}, f32[16,128]{1,0:T(8,128)S(1)}) custom-call(bf16[2048,128]{1,0:T(8,128)(2,1)} %heads.1, bf16[256,128]{1,0:T(8,128)(2,1)S(1)} %constant_dynamic-slice_fusion.factor), custom_call_target="tpu_custom_call" | custom-call | flops 200000000 | tf_op jit(solution)/shard_map/partial_first/pallas_call | solution.py:226
  16.5 7.2 %collective-permute-done.2 = f16[144,256]{1,0:T(8,128)(2,1)} collective-permute-done((f16[144,256]{1,0:T(8,128)(2,1)S(1)}, f16[144,256]{1,0:T(8,128)(2,1)}, u32[]{:S(2)}, u32[]{:S(2)}) %collective-permute-start.2) | collective-permute-done | bytes 73760 | tf_op jit(solution)/shard_map/ppermute | solution.py:20
  23.8 1.6 %collective-permute-start = (f16[144,256]{1,0:T(8,128)(2,1)S(1)}, f16[144,256]{1,0:T(8,128)(2,1)S(1)}, u32[]{:S(2)}, u32[]{:S(2)}) collective-permute-start(f16[144,256]{1,0:T(8,128)(2,1)S(1)} %convert_element_type.107), channel_id=1, source_target_pairs={{0,8},{8,0},{16,24},{24,16},{1,9},{9,1},{17,25},{25,17},{2,10},{10... | collective-permute-start | bytes 221192 | tf_op jit(solution)/shard_map/ppermute | solution.py:20
  26.8 1.5 %partial_second.1 = (f32[256,128]{1,0:T(8,128)S(1)}, f32[528,128]{1,0:T(8,128)S(1)}, f32[272,128]{1,0:T(8,128)S(1)}, f32[16,128]{1,0:T(8,128)S(1)}) custom-call(bf16[2048,128]{1,0:T(8,128)(2,1)} %collective-permute-done.3.heads, f32[1024,128]{1,0:T(8,128)S(1)} %get-tuple-element.16.parts, f32[16,128]{1,0:T(8,128)S(1)} %get-tuple-element.17.rows, ...), custom_call_target="tpu_custom_call" | custom-call | flops 200000000 | tf_op jit(solution)/shard_map/partial_second/pallas_call | solution.py:238
  28.3 1.6 %collective-permute-start.5 = (f16[528,128]{1,0:T(8,128)(2,1)S(1)}, f16[528,128]{1,0:T(8,128)(2,1)S(1)}, u32[]{:S(2)}, u32[]{:S(2)}) collective-permute-start(f16[528,128]{1,0:T(8,128)(2,1)S(1)} %convert_element_type.120), channel_id=1, source_target_pairs={{0,2},{1,7},{2,0},{3,5},{4,6},{5,3},{6,4},{7,1},{8,10},{9,15},{10,... | collective-permute-start | bytes 405512 | tf_op jit(solution)/shard_map/ppermute | solution.py:24
  30.0 2.6 %collective-permute-start.4 = (f16[272,128]{1,0:T(8,128)(2,1)S(1)}, f16[272,128]{1,0:T(8,128)(2,1)S(1)}, u32[]{:S(2)}, u32[]{:S(2)}) collective-permute-start(f16[272,128]{1,0:T(8,128)(2,1)S(1)} %convert_element_type.116), channel_id=1, source_target_pairs={{0,4},{1,5},{2,6},{3,7},{4,0},{5,1},{6,2},{7,3},{8,12},{9,13},{10,... | collective-permute-start | bytes 208904 | tf_op jit(solution)/shard_map/ppermute | solution.py:20
  32.6 2.7 %collective-permute-done.5 = f16[528,128]{1,0:T(8,128)(2,1)S(1)} collective-permute-done((f16[528,128]{1,0:T(8,128)(2,1)S(1)}, f16[528,128]{1,0:T(8,128)(2,1)S(1)}, u32[]{:S(2)}, u32[]{:S(2)}) %collective-permute-start.5) | collective-permute-done | bytes 135200 | tf_op jit(solution)/shard_map/ppermute | solution.py:24
  37.1 1.0 %slice.153 = f32[256,256]{1,0:T(8,128)S(1)} slice(f32[512,256]{1,0:T(8,128)} %collective-permute-done.21.refs_9_), slice={[0:256], [0:256]} | slice | bytes 524288 | tf_op jit(solution)/shard_map/slice | solution.py:343
  38.1 1.5 %collective-permute-start.23 = (f32[256,256]{1,0:T(8,128)S(1)}, f32[256,256]{1,0:T(8,128)S(1)}, u32[]{:S(2)}, u32[]{:S(2)}) collective-permute-start(f32[256,256]{1,0:T(8,128)S(1)} %slice.153), channel_id=1, source_target_pairs={{0,16},{8,24},{16,0},{24,8},{1,17},{9,25},{17,1},{25,9},{2,18},{10... | collective-permute-start | bytes 786440 | tf_op jit(solution)/shard_map/ppermute | solution.py:20
  39.7 2.5 %collective-permute-start.12 = (f16[256,128]{1,0:T(8,128)(2,1)S(1)}, f16[256,128]{1,0:T(8,128)(2,1)S(1)}, u32[]{:S(2)}, u32[]{:S(2)}) collective-permute-start(f16[256,128]{1,0:T(8,128)(2,1)S(1)} %multiply_convert_fusion), channel_id=1, source_target_pairs={{0,6},{1,7},{2,4},{3,5},{4,2},{5,3},{6,0},{7,1},{8,14},{9,15},{10,... | collective-permute-start | bytes 196616 | tf_op jit(solution)/shard_map/ppermute | solution.py:20
  42.2 2.0 %collective-permute-start.8 = (f16[256,128]{1,0:T(8,128)(2,1)S(1)}, f16[256,128]{1,0:T(8,128)(2,1)S(1)}, u32[]{:S(2)}, u32[]{:S(2)}) collective-permute-start(f16[256,128]{1,0:T(8,128)(2,1)S(1)} %multiply_convert_fusion), channel_id=1, source_target_pairs={{0,2},{1,3},{2,0},{3,1},{4,6},{5,7},{6,4},{7,5},{8,10},{9,11},{10,... | collective-permute-start | bytes 196616 | tf_op jit(solution)/shard_map/ppermute | solution.py:20
  44.4 4.2 %collective-permute-done.10 = f16[256,128]{1,0:T(8,128)(2,1)S(1)} collective-permute-done((f16[256,128]{1,0:T(8,128)(2,1)S(1)}, f16[256,128]{1,0:T(8,128)(2,1)S(1)}, u32[]{:S(2)}, u32[]{:S(2)}) %collective-permute-start.10) | collective-permute-done | bytes 65568 | tf_op jit(solution)/shard_map/ppermute | solution.py:20
  52.0 1.5 %collective-permute-start.16 = (f16[144,256]{1,0:T(8,128)(2,1)S(1)}, f16[144,256]{1,0:T(8,128)(2,1)S(1)}, u32[]{:S(2)}, u32[]{:S(2)}) collective-permute-start(f16[144,256]{1,0:T(8,128)(2,1)S(1)} %convert_element_type.128), channel_id=1, source_target_pairs={{0,24},{8,16},{16,8},{24,0},{1,25},{9,17},{17,9},{25,1},{2,26},{10... | collective-permute-start | bytes 221192 | tf_op jit(solution)/shard_map/ppermute | solution.py:20
  53.5 1.5 %collective-permute-start.15 = (f16[144,256]{1,0:T(8,128)(2,1)S(1)}, f16[144,256]{1,0:T(8,128)(2,1)S(1)}, u32[]{:S(2)}, u32[]{:S(2)}) collective-permute-start(f16[144,256]{1,0:T(8,128)(2,1)S(1)} %convert_element_type.128), channel_id=1, source_target_pairs={{0,16},{8,24},{16,0},{24,8},{1,17},{9,25},{17,1},{25,9},{2,18},{10... | collective-permute-start | bytes 221192 | tf_op jit(solution)/shard_map/ppermute | solution.py:20
  55.6 1.9 %collective-permute-done.16 = f16[144,256]{1,0:T(8,128)(2,1)S(1)} collective-permute-done((f16[144,256]{1,0:T(8,128)(2,1)S(1)}, f16[144,256]{1,0:T(8,128)(2,1)S(1)}, u32[]{:S(2)}, u32[]{:S(2)}) %collective-permute-start.16) | collective-permute-done | bytes 73760 | tf_op jit(solution)/shard_map/ppermute | solution.py:20
  57.5 1.4 %collective-permute-done.15 = f16[144,256]{1,0:T(8,128)(2,1)S(1)} collective-permute-done((f16[144,256]{1,0:T(8,128)(2,1)S(1)}, f16[144,256]{1,0:T(8,128)(2,1)S(1)}, u32[]{:S(2)}, u32[]{:S(2)}) %collective-permute-start.15) | collective-permute-done | bytes 73760 | tf_op jit(solution)/shard_map/ppermute | solution.py:20
  59.6 1.2 %collective-permute-done.17.b = f32[8,128]{1,0:T(8,128)S(1)} collective-permute-done((f32[8,128]{1,0:T(8,128)S(1)}, f32[8,128]{1,0:T(8,128)S(1)}, u32[]{:S(2)}, u32[]{:S(2)}) %collective-permute-start.17) | collective-permute-done | bytes 4128 | tf_op jit(solution)/shard_map/ppermute | solution.py:20
  60.8 2.9 %collective-permute-start.19 = (f32[8,128]{1,0:T(8,128)S(1)}, f32[8,128]{1,0:T(8,128)S(1)}, u32[]{:S(2)}, u32[]{:S(2)}) collective-permute-start(f32[8,128]{1,0:T(8,128)S(1)} %add_tiles.1.refs_0_), channel_id=1, source_target_pairs={{0,4},{1,5},{2,6},{3,7},{4,0},{5,1},{6,2},{7,3},{8,12},{9,13},{10,... | collective-permute-start | bytes 12296 | tf_op jit(solution)/shard_map/ppermute | solution.py:20
  66.0 2.8 %finish.1 = (f32[128,256]{1,0:T(8,128)}, f32[128,256]{1,0:T(8,128)}, bf16[512,256]{1,0:T(8,128)(2,1)}, f32[32,256]{1,0:T(8,128)}, f32[32,256]{1,0:T(8,128)}, /*i...) custom-call(f32[8,128]{1,0:T(8,128)S(1)} %add_tiles.1.refs_0_, ...), custom_call_target="tpu_custom_call" | custom-call | tf_op jit(solution)/shard_map/finish/pallas_call | solution.py:105
  (86 shorter events, 15.3 us)
Async XLA Ops:
  5.7 30.7 %collective-permute-start.22 = (f32[512,256]{1,0:T(8,128)S(1)}, f32[512,256]{1,0:T(8,128)S(1)}, u32[]{:S(2)}, u32[]{:S(2)}) collective-permute-start(f32[512,256]{1,0:T(8,128)S(1)} %pack_rows.1.refs_8_), channel_id=1, source_target_pairs={{0,16},{8,24},{16,0},{24,8},{1,17},{9,25},{17,1},{25,9},{2,18},{10... | collective-permute-start | bytes 1572872 | tf_op jit(solution)/shard_map/ppermute | solution.py:20
  8.8 28.3 %collective-permute-start.21 = (f32[512,256]{1,0:T(8,128)S(1)}, f32[512,256]{1,0:T(8,128)}, u32[]{:S(2)}, u32[]{:S(2)}) collective-permute-start(f32[512,256]{1,0:T(8,128)S(1)} %pack_rows.1.refs_8_), channel_id=1, source_target_pairs={{0,8},{8,0},{16,24},{24,16},{1,9},{9,1},{17,25},{25,17},{2,10},{10... | collective-permute-start | bytes 1572872 | tf_op jit(solution)/shard_map/ppermute | solution.py:20
  12.8 11.0 %collective-permute-start.2 = (f16[144,256]{1,0:T(8,128)(2,1)S(1)}, f16[144,256]{1,0:T(8,128)(2,1)}, u32[]{:S(2)}, u32[]{:S(2)}) collective-permute-start(f16[144,256]{1,0:T(8,128)(2,1)S(1)} %convert_element_type.107), channel_id=1, source_target_pairs={{0,24},{8,16},{16,8},{24,0},{1,25},{9,17},{17,9},{25,1},{2,26},{10... | collective-permute-start | bytes 221192 | tf_op jit(solution)/shard_map/ppermute | solution.py:20
  12.9 13.2 %collective-permute-start.1 = (f16[144,256]{1,0:T(8,128)(2,1)S(1)}, f16[144,256]{1,0:T(8,128)(2,1)}, u32[]{:S(2)}, u32[]{:S(2)}) collective-permute-start(f16[144,256]{1,0:T(8,128)(2,1)S(1)} %convert_element_type.107), channel_id=1, source_target_pairs={{0,16},{8,24},{16,0},{24,8},{1,17},{9,25},{17,1},{25,9},{2,18},{10... | collective-permute-start | bytes 221192 | tf_op jit(solution)/shard_map/ppermute | solution.py:20
  14.9 11.9 %collective-permute-start.3 = (bf16[2048,128]{1,0:T(8,128)(2,1)}, bf16[2048,128]{1,0:T(8,128)(2,1)}, u32[]{:S(2)}, u32[]{:S(2)}) collective-permute-start(bf16[2048,128]{1,0:T(8,128)(2,1)} %heads.1), channel_id=1, source_target_pairs={{0,1},{1,0},{2,3},{3,2},{4,5},{5,4},{6,7},{7,6},{8,9},{9,8},{10,11... | collective-permute-start | bytes 1572872 | tf_op jit(solution)/shard_map/ppermute | solution.py:20
  23.8 6.2 %collective-permute-start = (f16[144,256]{1,0:T(8,128)(2,1)S(1)}, f16[144,256]{1,0:T(8,128)(2,1)S(1)}, u32[]{:S(2)}, u32[]{:S(2)}) collective-permute-start(f16[144,256]{1,0:T(8,128)(2,1)S(1)} %convert_element_type.107), channel_id=1, source_target_pairs={{0,8},{8,0},{16,24},{24,16},{1,9},{9,1},{17,25},{25,17},{2,10},{10... | collective-permute-start | bytes 221192 | tf_op jit(solution)/shard_map/ppermute | solution.py:20
  28.3 7.0 %collective-permute-start.5 = (f16[528,128]{1,0:T(8,128)(2,1)S(1)}, f16[528,128]{1,0:T(8,128)(2,1)S(1)}, u32[]{:S(2)}, u32[]{:S(2)}) collective-permute-start(f16[528,128]{1,0:T(8,128)(2,1)S(1)} %convert_element_type.120), channel_id=1, source_target_pairs={{0,2},{1,7},{2,0},{3,5},{4,6},{5,3},{6,4},{7,1},{8,10},{9,15},{10,... | collective-permute-start | bytes 405512 | tf_op jit(solution)/shard_map/ppermute | solution.py:24
  30.0 9.6 %collective-permute-start.4 = (f16[272,128]{1,0:T(8,128)(2,1)S(1)}, f16[272,128]{1,0:T(8,128)(2,1)S(1)}, u32[]{:S(2)}, u32[]{:S(2)}) collective-permute-start(f16[272,128]{1,0:T(8,128)(2,1)S(1)} %convert_element_type.116), channel_id=1, source_target_pairs={{0,4},{1,5},{2,6},{3,7},{4,0},{5,1},{6,2},{7,3},{8,12},{9,13},{10,... | collective-permute-start | bytes 208904 | tf_op jit(solution)/shard_map/ppermute | solution.py:20
  35.4 4.2 %collective-permute-start.6 = (f16[272,128]{1,0:T(8,128)(2,1)S(1)}, f16[272,128]{1,0:T(8,128)(2,1)S(1)}, u32[]{:S(2)}, u32[]{:S(2)}) collective-permute-start(f16[272,128]{1,0:T(8,128)(2,1)S(1)} %slice.138), channel_id=1, source_target_pairs={{0,1},{1,0},{2,3},{3,2},{4,5},{5,4},{6,7},{7,6},{8,9},{9,8},{10,11... | collective-permute-start | bytes 208904 | tf_op jit(solution)/shard_map/ppermute | solution.py:20
  36.4 28.8 %collective-permute-start.24 = (f32[256,256]{1,0:T(8,128)S(1)}, f32[256,256]{1,0:T(8,128)S(1)}, u32[]{:S(2)}, u32[]{:S(2)}) collective-permute-start(f32[256,256]{1,0:T(8,128)S(1)} %slice.154), channel_id=1, source_target_pairs={{0,8},{8,0},{16,24},{24,16},{1,9},{9,1},{17,25},{25,17},{2,10},{10... | collective-permute-start | bytes 786440 | tf_op jit(solution)/shard_map/ppermute | solution.py:20
  38.1 27.1 %collective-permute-start.23 = (f32[256,256]{1,0:T(8,128)S(1)}, f32[256,256]{1,0:T(8,128)S(1)}, u32[]{:S(2)}, u32[]{:S(2)}) collective-permute-start(f32[256,256]{1,0:T(8,128)S(1)} %slice.153), channel_id=1, source_target_pairs={{0,16},{8,24},{16,0},{24,8},{1,17},{9,25},{17,1},{25,9},{2,18},{10... | collective-permute-start | bytes 786440 | tf_op jit(solution)/shard_map/ppermute | solution.py:20
  39.7 9.1 %collective-permute-start.12 = (f16[256,128]{1,0:T(8,128)(2,1)S(1)}, f16[256,128]{1,0:T(8,128)(2,1)S(1)}, u32[]{:S(2)}, u32[]{:S(2)}) collective-permute-start(f16[256,128]{1,0:T(8,128)(2,1)S(1)} %multiply_convert_fusion), channel_id=1, source_target_pairs={{0,6},{1,7},{2,4},{3,5},{4,2},{5,3},{6,0},{7,1},{8,14},{9,15},{10,... | collective-permute-start | bytes 196616 | tf_op jit(solution)/shard_map/ppermute | solution.py:20
  42.2 6.4 %collective-permute-start.10 = (f16[256,128]{1,0:T(8,128)(2,1)S(1)}, f16[256,128]{1,0:T(8,128)(2,1)S(1)}, u32[]{:S(2)}, u32[]{:S(2)}) collective-permute-start(f16[256,128]{1,0:T(8,128)(2,1)S(1)} %multiply_convert_fusion), channel_id=1, source_target_pairs={{0,4},{1,5},{2,6},{3,7},{4,0},{5,1},{6,2},{7,3},{8,12},{9,13},{10,... | collective-permute-start | bytes 196616 | tf_op jit(solution)/shard_map/ppermute | solution.py:20
  42.2 7.2 %collective-permute-start.8 = (f16[256,128]{1,0:T(8,128)(2,1)S(1)}, f16[256,128]{1,0:T(8,128)(2,1)S(1)}, u32[]{:S(2)}, u32[]{:S(2)}) collective-permute-start(f16[256,128]{1,0:T(8,128)(2,1)S(1)} %multiply_convert_fusion), channel_id=1, source_target_pairs={{0,2},{1,3},{2,0},{3,1},{4,6},{5,7},{6,4},{7,5},{8,10},{9,11},{10,... | collective-permute-start | bytes 196616 | tf_op jit(solution)/shard_map/ppermute | solution.py:20
  48.5 1.3 %collective-permute-start.7 = (f16[256,128]{1,0:T(8,128)(2,1)S(1)}, f16[256,128]{1,0:T(8,128)(2,1)S(1)}, u32[]{:S(2)}, u32[]{:S(2)}) collective-permute-start(f16[256,128]{1,0:T(8,128)(2,1)S(1)} %multiply_convert_fusion), channel_id=1, source_target_pairs={{0,1},{1,0},{2,3},{3,2},{4,5},{5,4},{6,7},{7,6},{8,9},{9,8},{10,11... | collective-permute-start | bytes 196616 | tf_op jit(solution)/shard_map/ppermute | solution.py:20
  48.8 2.5 %collective-permute-start.11 = (f16[256,128]{1,0:T(8,128)(2,1)S(1)}, f16[256,128]{1,0:T(8,128)(2,1)S(1)}, u32[]{:S(2)}, u32[]{:S(2)}) collective-permute-start(f16[256,128]{1,0:T(8,128)(2,1)S(1)} %collective-permute-done.10), channel_id=1, source_target_pairs={{0,1},{1,0},{2,3},{3,2},{4,5},{5,4},{6,7},{7,6},{8,9},{9,8},{10,11... | collective-permute-start | bytes 196616 | tf_op jit(solution)/shard_map/ppermute | solution.py:20
  49.4 2.2 %collective-permute-start.13 = (f16[256,128]{1,0:T(8,128)(2,1)S(1)}, f16[256,128]{1,0:T(8,128)(2,1)S(1)}, u32[]{:S(2)}, u32[]{:S(2)}) collective-permute-start(f16[256,128]{1,0:T(8,128)(2,1)S(1)} %collective-permute-done.12), channel_id=1, source_target_pairs={{0,1},{1,0},{2,3},{3,2},{4,5},{5,4},{6,7},{7,6},{8,9},{9,8},{10,11... | collective-permute-start | bytes 196616 | tf_op jit(solution)/shard_map/ppermute | solution.py:20
  49.8 1.3 %collective-permute-start.9 = (f16[256,128]{1,0:T(8,128)(2,1)S(1)}, f16[256,128]{1,0:T(8,128)(2,1)S(1)}, u32[]{:S(2)}, u32[]{:S(2)}) collective-permute-start(f16[256,128]{1,0:T(8,128)(2,1)S(1)} %collective-permute-done.8), channel_id=1, source_target_pairs={{0,1},{1,0},{2,3},{3,2},{4,5},{5,4},{6,7},{7,6},{8,9},{9,8},{10,11... | collective-permute-start | bytes 196616 | tf_op jit(solution)/shard_map/ppermute | solution.py:20
  52.0 5.5 %collective-permute-start.16 = (f16[144,256]{1,0:T(8,128)(2,1)S(1)}, f16[144,256]{1,0:T(8,128)(2,1)S(1)}, u32[]{:S(2)}, u32[]{:S(2)}) collective-permute-start(f16[144,256]{1,0:T(8,128)(2,1)S(1)} %convert_element_type.128), channel_id=1, source_target_pairs={{0,24},{8,16},{16,8},{24,0},{1,25},{9,17},{17,9},{25,1},{2,26},{10... | collective-permute-start | bytes 221192 | tf_op jit(solution)/shard_map/ppermute | solution.py:20
  53.5 5.4 %collective-permute-start.15 = (f16[144,256]{1,0:T(8,128)(2,1)S(1)}, f16[144,256]{1,0:T(8,128)(2,1)S(1)}, u32[]{:S(2)}, u32[]{:S(2)}) collective-permute-start(f16[144,256]{1,0:T(8,128)(2,1)S(1)} %convert_element_type.128), channel_id=1, source_target_pairs={{0,16},{8,24},{16,0},{24,8},{1,17},{9,25},{17,1},{25,9},{2,18},{10... | collective-permute-start | bytes 221192 | tf_op jit(solution)/shard_map/ppermute | solution.py:20
  55.1 4.4 %collective-permute-start.14 = (f16[144,256]{1,0:T(8,128)(2,1)S(1)}, f16[144,256]{1,0:T(8,128)(2,1)S(1)}, u32[]{:S(2)}, u32[]{:S(2)}) collective-permute-start(f16[144,256]{1,0:T(8,128)(2,1)S(1)} %convert_element_type.128), channel_id=1, source_target_pairs={{0,8},{8,0},{16,24},{24,16},{1,9},{9,1},{17,25},{25,17},{2,10},{10... | collective-permute-start | bytes 221192 | tf_op jit(solution)/shard_map/ppermute | solution.py:20
  60.8 3.6 %collective-permute-start.18 = (f32[8,128]{1,0:T(8,128)S(1)}, f32[8,128]{1,0:T(8,128)S(1)}, u32[]{:S(2)}, u32[]{:S(2)}) collective-permute-start(f32[8,128]{1,0:T(8,128)S(1)} %add_tiles.1.refs_0_), channel_id=1, source_target_pairs={{0,2},{1,7},{2,0},{3,5},{4,6},{5,3},{6,4},{7,1},{8,10},{9,15},{10,... | collective-permute-start | bytes 12296 | tf_op jit(solution)/shard_map/ppermute | solution.py:24
  60.8 4.5 %collective-permute-start.19 = (f32[8,128]{1,0:T(8,128)S(1)}, f32[8,128]{1,0:T(8,128)S(1)}, u32[]{:S(2)}, u32[]{:S(2)}) collective-permute-start(f32[8,128]{1,0:T(8,128)S(1)} %add_tiles.1.refs_0_), channel_id=1, source_target_pairs={{0,4},{1,5},{2,6},{3,7},{4,0},{5,1},{6,2},{7,3},{8,12},{9,13},{10,... | collective-permute-start | bytes 12296 | tf_op jit(solution)/shard_map/ppermute | solution.py:20
  64.4 1.6 %collective-permute-start.20 = (f32[8,128]{1,0:T(8,128)S(1)}, f32[8,128]{1,0:T(8,128)S(1)}, u32[]{:S(2)}, u32[]{:S(2)}) collective-permute-start(f32[8,128]{1,0:T(8,128)S(1)} %collective-permute-done.18.refs_1_), channel_id=1, source_target_pairs={{0,1},{1,0},{2,3},{3,2},{4,5},{5,4},{6,7},{7,6},{8,9},{9,8},{10,11... | collective-permute-start | bytes 12296 | tf_op jit(solution)/shard_map/ppermute | solution.py:20
  (12 other events, 71.4 us)
